TPU v7x, 256 devices: a whole 4x4x8 slice. The times are simulated.
256 devices in a mesh: sp: 16 (over y, x), dp: 16 (over z, core).
Axes of the slice: x: 4, y: 4, z: 8, core: 2. Of those that a mesh axis runs over, the one named last changes fastest.
Arguments:
- tokens: bfloat16 [16, 5120, 2048], P('dp', 'sp'), may hold values from -6 to 6
- up_weight: bfloat16 [2048, 2048], P('dp'), may hold values from -0.125 to 0.125
- gate_weight: bfloat16 [2048, 2048], P('dp'), may hold values from -0.125 to 0.125
- group_gain: float32 [16, 128], P('sp'), may hold values from 0.1 to 1.9
- mix_weight: bfloat16 [16, 1280, 1280], P('sp', 'dp'), may hold values from -0.15625 to 0.15625
- mix_bias: float32 [16, 1280], P('sp'), may hold values from 0.5 to 1.5
- out_gain: float32 [2048], replicated, may hold values from 0.1 to 1.9
- out_weight: bfloat16 [2048, 2048], P(None, 'dp'), may hold values from -0.125 to 0.125
Outputs:
- mixed_out: bfloat16 [16, 5120, 2048], P('dp', 'sp')
All inputs are finite; a program needn't handle non-finite values.
Results may differ from a plain program's by a relative error of at most 0.0072.
Values may be sent and summed in bfloat16 or wider, within the bound.
A program may use at most 128 MiB of HBM per device.

v0:
```python
import jax
import jax.numpy as jnp
from jax import lax
from jax.sharding import PartitionSpec as P

norm_eps = 1e-06


def in_one_piece(arrays, axis, dim, along):
    widths = [a.shape[along] for a in arrays]
    both = jnp.concatenate(arrays, axis=along)
    result = lax.all_gather(both, axis, axis=dim, tiled=True)
    return tuple(jnp.split(result, [sum(widths[:k]) for k in range(1, len(widths))], axis=along))


def laid_out(pieces, dim):
    lengths = list(pieces.shape[1:])
    lengths[dim] *= pieces.shape[0]
    return jnp.moveaxis(pieces, 0, dim).reshape(lengths)


def on_gathered_pieces(x, axis, dim, work, out_dim):
    rows = x.shape[dim]
    pieces = jnp.split(x, 2, axis=dim) if rows % 2 == 0 else [x]
    initial = jnp.arange(lax.axis_size(axis)) * rows
    blocks = [lax.all_gather(piece, axis) for piece in pieces]
    made = [jax.vmap(work)(b, initial + k * (rows // len(pieces))) for k, b in enumerate(blocks)]
    return laid_out(jnp.concatenate(made, axis=out_dim + 1), out_dim)


def body(tokens, up_weight, gate_weight, group_gain, mix_weight, mix_bias, out_gain, out_weight):
    sequences, per_device, model_width = tokens.shape
    groups_dev, group_dim = group_gain.shape
    groups = groups_dev * lax.axis_size("sp")
    mix_width = groups * group_dim
    flat_rows = tokens.reshape(sequences * per_device, model_width)
    full_mix = lax.all_gather(mix_weight, "dp", axis=1, tiled=True)
    block_len = full_mix.shape[1]
    lower = jnp.tril(jnp.ones((block_len, block_len), dtype=bool))
    masked_mix = jnp.where(lower[None], full_mix, jnp.zeros_like(full_mix))
    bias_cols = mix_bias.T

    def contract(shard_rows):
        return jnp.dot(flat_rows, shard_rows, preferred_element_type=jnp.float32)

    def by_group(product):
        return product.astype(jnp.bfloat16).reshape(sequences, per_device, groups, group_dim)

    shard_pair = in_one_piece((up_weight, gate_weight), "dp", 0, 1)
    up_proj = contract(shard_pair[0])
    gate_proj = contract(shard_pair[1])
    up_heads = lax.all_to_all(by_group(up_proj), "sp", split_axis=2, concat_axis=1, tiled=True)
    gate_heads = lax.all_to_all(by_group(gate_proj), "sp", split_axis=2, concat_axis=1, tiled=True)
    members = up_heads.shape[0]
    seq_len = up_heads.shape[1]
    opened = jax.nn.gelu(up_heads.astype(jnp.float32))
    gate_act = jax.nn.gelu(gate_heads.astype(jnp.float32))
    center = jnp.mean(gate_act, axis=-1, keepdims=True)
    spread = jnp.mean(jnp.square(gate_act - center), axis=-1, keepdims=True)
    normal_v = ((gate_act - center) * lax.rsqrt(spread + norm_eps) * group_gain).astype(
        jnp.bfloat16
    )
    blocks = normal_v.reshape(members, seq_len // block_len, block_len, groups_dev, group_dim)
    mixed_sum = jnp.einsum(
        "gij,snjgc->snigc", masked_mix, blocks, preferred_element_type=jnp.float32
    )
    mixed_sum = mixed_sum + bias_cols[None, None, :, :, None]
    gated = (opened * mixed_sum.reshape(members, seq_len, groups_dev, group_dim)).astype(
        jnp.bfloat16
    )
    by_token = lax.all_to_all(gated, "sp", split_axis=1, concat_axis=2, tiled=True)
    gated_f = by_token.reshape(sequences * per_device, mix_width).astype(jnp.float32)
    scale = lax.rsqrt(jnp.mean(gated_f * gated_f, axis=-1, keepdims=True) + norm_eps)
    normed = (gated_f * scale * out_gain).astype(jnp.bfloat16)

    def project(shard_cols, offset):
        return jnp.dot(normed, shard_cols, preferred_element_type=jnp.float32)

    output = on_gathered_pieces(out_weight, "dp", 1, project, 1)
    return output.astype(jnp.bfloat16).reshape(sequences, per_device, model_width)


def solution(mesh):
    return jax.shard_map(
        body,
        mesh=mesh,
        in_specs=(
            P("dp", "sp", None),
            P("dp", None),
            P("dp", None),
            P("sp", None),
            P("sp", "dp", None),
            P("sp", None),
            P(),
            P(None, "dp"),
        ),
        out_specs=P("dp", "sp", None),
        check_vma=False,
    )
```

profile of v0, /device:TPU:1, one launch (start us, length us, event | category | flops | bytes accessed | tf_op | source)
XLA Modules:
  0.0 294.0 jit_solution(13342779105708526144)
XLA Ops:
  6.5 2.4 pad_maximum_fusion.1
  9.0 0.7 all-gather.9.cloned.1.call-update
  9.8 1.2 fusion.77
  11.6 97.2 %all-gather.7.cloned.1.call-done = bf16[2048,4096]{1,0:T(8,128)(2,1)} async-done(((bf16[128,4096]{1,0:T(8,128)(2,1)}), bf16[2048,4096]{1,0:T(8,128)(2,1)}) %all-gather.7.cloned.1.call-update) | async-done | bytes 16777232 | tf_op jit(solution)/shard_map/all_gather | solution.py:12
  108.7 6.3 %fusion.64 = bf16[40,8,16,128]{3,1,2,0:T(8,128)(2,1)S(1)} fusion(bf16[2048,4096]{1,0:T(8,128)(2,1)} %all-gather.7.cloned.1.call-done, bf16[1,320,2048]{2,1,0:T(8,128)(2,1)S(1)} %copy-done), kind=kOutput, calls=%fused_computation.61 | convolution fusion | flops 2685009920 | bytes 11010048 | tf_op jit(solution)/shard_map/dot_general | solution.py:44
  115.3 1.4 copy.45
  116.7 6.5 %all-to-all-start.1 = ((bf16[1,320,16,128]{3,1,0,2:T(8,128)(2,1)}), bf16[1,320,16,128]{3,1,0,2:T(8,128)(2,1)S(1)}, u32[]{:S(2)}, u32[]{:S(2)}) async-start(bf16[1,320,16,128]{3,1,0,2:T(8,128)(2,1)} %copy.45), calls=%async_computation.1 | async-start | bytes 2621440 | tf_op jit(solution)/shard_map/all_to_all | solution.py:53
  123.3 6.4 %fusion.67 = bf16[40,8,16,128]{3,1,2,0:T(8,128)(2,1)S(1)} fusion(bf16[2048,4096]{1,0:T(8,128)(2,1)} %all-gather.7.cloned.1.call-done, bf16[1,320,2048]{2,1,0:T(8,128)(2,1)S(1)} %copy-done), kind=kOutput, calls=%fused_computation.62 | convolution fusion | flops 2685009920 | bytes 11010048 | tf_op jit(solution)/shard_map/dot_general | solution.py:44
  130.0 1.4 copy.43
  131.4 12.5 %all-to-all-done.1 = bf16[1,320,16,128]{3,1,0,2:T(8,128)(2,1)S(1)} async-done(((bf16[1,320,16,128]{3,1,0,2:T(8,128)(2,1)}), bf16[1,320,16,128]{3,1,0,2:T(8,128)(2,1)S(1)}, u32[]{:S(2)}, u32[]{:S(2)}) %all-to-all-start.1) | async-done | bytes 1310752 | tf_op jit(solution)/shard_map/all_to_all | solution.py:53
  143.8 4.6 %all-to-all-start = ((bf16[1,320,16,128]{3,1,0,2:T(8,128)(2,1)}), bf16[1,320,16,128]{3,1,0,2:T(8,128)(2,1)}, u32[]{:S(2)}, u32[]{:S(2)}) async-start(bf16[1,320,16,128]{3,1,0,2:T(8,128)(2,1)} %copy.43), calls=%async_computation | async-start | bytes 2621440 | tf_op jit(solution)/shard_map/all_to_all | solution.py:52
  148.4 1.1 fusion.61
  149.9 3.0 %fusion.62 = f32[5120]{0:T(1024)S(1)} fusion(f32[1,320,16,1,128]{4,1,2,3,0:T(8,128)S(1)} %bitcast_convert_fusion, f32[5120]{0:T(1024)S(1)} %div.15), kind=kLoop, calls=%fused_computation.58 | loop fusion | flops 7203840 | bytes 2662400 | tf_op jit(solution)/shard_map/reduce_sum | solution.py:59
  152.9 1.7 fusion.42
  154.7 5.4 %fusion.14 = f32[1,4,1280,1,128]{2,4,1,0,3:T(8,128)} fusion(bf16[4,1280,128]{2,1,0:T(8,128)(2,1)S(1)} %bitcast.118, bf16[1,1280,1280]{2,1,0:T(8,128)(2,1)} %all-gather.9.cloned.1.call-done, f32[1280]{0:T(1024)S(1)} %reduce.8), kind=kOutput, calls=%fused_computation.14 | convolution fusion | flops 1681653760 | bytes 7214080 | tf_op jit(solution)/shard_map/gij,snjgc->snigc/dot_general | solution.py:64
  160.1 2.3 copy.48
  162.4 3.9 %all-to-all-done = bf16[1,320,16,128]{3,1,0,2:T(8,128)(2,1)} async-done(((bf16[1,320,16,128]{3,1,0,2:T(8,128)(2,1)}), bf16[1,320,16,128]{3,1,0,2:T(8,128)(2,1)}, u32[]{:S(2)}, u32[]{:S(2)}) %all-to-all-start) | async-done | bytes 1310752 | tf_op jit(solution)/shard_map/all_to_all | solution.py:52
  166.3 1.6 bitcast_convert_fusion.1
  167.9 0.9 fusion.31
  168.9 20.9 %copy.72 = bf16[1,5120,1,128]{3,2,0,1:T(2,128)(2,1)S(1)} copy(bf16[1,5120,1,128]{3,1,2,0:T(8,128)(2,1)S(1)} %fusion.31) | data formatting | bytes 2621440 | tf_op jit(solution)/shard_map/convert_element_type | solution.py:68
  190.3 28.8 %reduce.9 = bf16[5120,128]{1,0:T(8,128)(2,1)} reduce(bf16[5120,1,1,128]{3,2,1,0:T(2,128)(2,1)S(1)} %bitcast.106, bf16[]{:T(256)} %broadcast.309), dimensions={1,2}, to_apply=%bitcast.101.reduce_sub_computation | reduce | bytes 2621442
  219.1 4.1 %reshape.409 = bf16[16,2,20480]{2,1,0:T(2,128)(2,1)} reshape(bf16[5120,128]{1,0:T(8,128)(2,1)} %reduce.9) | data formatting | bytes 2621440
  223.1 4.7 %all-to-all-start.2 = ((bf16[16,2,20480]{2,1,0:T(2,128)(2,1)}), bf16[16,2,20480]{2,1,0:T(2,128)(2,1)}, u32[]{:S(2)}, u32[]{:S(2)}) async-start(bf16[16,2,20480]{2,1,0:T(2,128)(2,1)} %reshape.409), calls=%async_computation.2 | async-start | bytes 2621440 | tf_op jit(solution)/shard_map/all_to_all | solution.py:71
  227.9 8.7 %copy.53 = bf16[16,2048,64]{1,2,0:T(8,128)(2,1)} copy(bf16[16,2048,64]{2,1,0:T(8,128)(2,1)} %bitcast.107) | data formatting | bytes 8388608 | tf_op jit(solution)/shard_map/all_gather | solution.py:26
  236.6 25.8 %all-gather.13.cloned.1.call-done = bf16[32768,64]{1,0:T(8,128)(2,1)} async-done(((bf16[2048,64]{1,0:T(8,128)(2,1)}), bf16[32768,64]{1,0:T(8,128)(2,1)}) %all-gather.13.cloned.1.call-update) | async-done | bytes 4194320 | tf_op jit(solution)/shard_map/all_gather | solution.py:26
  262.4 8.6 %copy.55 = bf16[16,2048,64]{1,2,0:T(8,128)(2,1)} copy(bf16[16,2048,64]{2,1,0:T(8,128)(2,1)} %bitcast.108) | data formatting | bytes 8388608 | tf_op jit(solution)/shard_map/all_gather | solution.py:26
  271.0 4.5 %reshape.410 = bf16[5120,1,1,128]{3,2,1,0:T(2,128)(2,1)S(1)} reshape(bf16[16,2,20480]{2,1,0:T(2,128)(2,1)} %all-to-all-done.2) | data formatting | bytes 2621440
  275.7 0.7 multiply_reduce_fusion
  276.4 1.5 copy.51
  278.1 4.8 %fusion.75 = f32[320,1024]{0,1:S(1)} fusion(bf16[2048,1024]{0,1:T(8,128)(2,1)} %bitcast.112, f32[40,8,16,128]{3,2,1,0:T(8,128)S(1)} %bitcast.114, f32[2048]{0:T(1024)S(1)} %copy-done.6, f32[320]{0:T(512)S(1)} %add_rsqrt_fusion.1), kind=kOutput, calls=%fused_computation.76 | convolution fusion | flops 1344143360 | bytes 8135936
  282.9 2.5 fusion.73
  285.9 1.5 copy.56
  (38 shorter events, 2.9 us)
Async XLA Ops:
  6.5 102.2 %copy-start = (bf16[1,320,2048]{2,1,0:T(8,128)(2,1)S(1)}, bf16[1,320,2048]{2,1,0:T(8,128)(2,1)}, u32[]{:S(2)}) copy-start(bf16[1,320,2048]{2,1,0:T(8,128)(2,1)} %param.8) | copy-start | bytes 3932164
  6.5 3.2 %copy-start.3 = (bf16[2048,128]{1,0:T(8,128)(2,1)S(1)}, bf16[2048,128]{1,0:T(8,128)(2,1)}, u32[]{:S(2)}) copy-start(bf16[2048,128]{1,0:T(8,128)(2,1)} %param.15) | copy-start | bytes 1572868
  6.5 102.2 %all-gather.7.cloned.1.call-start = ((), (), s32[]{:S(2)}) async-start(), calls=%async_computation.3 | async-start | bytes 17825792 | tf_op jit(solution)/shard_map/all_gather | solution.py:12
  9.0 145.7 %all-gather.9.cloned.1.call-start = ((), (), s32[]{:S(2)}) async-start(), calls=%async_computation.4 | async-start | bytes 3481600 | tf_op jit(solution)/shard_map/all_gather | solution.py:37
  9.7 218.2 %all-gather.11.cloned.1.call-start = ((), (), s32[]{:S(2)}) async-start(), calls=%async_computation.5 | async-start | bytes 8912896 | tf_op jit(solution)/shard_map/all_gather | solution.py:26
  11.0 251.4 %all-gather.13.cloned.1.call-start = ((), (), s32[]{:S(2)}) async-start(), calls=%async_computation.6 | async-start | bytes 8912896 | tf_op jit(solution)/shard_map/all_gather | solution.py:26
  115.3 7.9 %copy-start.4 = (f32[1,1280]{1,0:T(1,128)S(1)}, f32[1,1280]{1,0:T(1,128)}, u32[]{:S(2)}) copy-start(f32[1,1280]{1,0:T(1,128)} %param.13) | copy-start | bytes 15364
  116.7 27.1 %all-to-all-start.1 = ((bf16[1,320,16,128]{3,1,0,2:T(8,128)(2,1)}), bf16[1,320,16,128]{3,1,0,2:T(8,128)(2,1)S(1)}, u32[]{:S(2)}, u32[]{:S(2)}) async-start(bf16[1,320,16,128]{3,1,0,2:T(8,128)(2,1)} %copy.45), calls=%async_computation.1 | async-start | bytes 2621440 | tf_op jit(solution)/shard_map/all_to_all | solution.py:53
  143.8 22.5 %all-to-all-start = ((bf16[1,320,16,128]{3,1,0,2:T(8,128)(2,1)}), bf16[1,320,16,128]{3,1,0,2:T(8,128)(2,1)}, u32[]{:S(2)}, u32[]{:S(2)}) async-start(bf16[1,320,16,128]{3,1,0,2:T(8,128)(2,1)} %copy.43), calls=%async_computation | async-start | bytes 2621440 | tf_op jit(solution)/shard_map/all_to_all | solution.py:52
  149.6 3.3 %copy-start.5 = (f32[1,128]{1,0:T(1,128)S(1)}, f32[1,128]{1,0:T(1,128)}, u32[]{:S(2)}) copy-start(f32[1,128]{1,0:T(1,128)} %param.11) | copy-start | bytes 1540
  223.1 47.8 %all-to-all-start.2 = ((bf16[16,2,20480]{2,1,0:T(2,128)(2,1)}), bf16[16,2,20480]{2,1,0:T(2,128)(2,1)}, u32[]{:S(2)}, u32[]{:S(2)}) async-start(bf16[16,2,20480]{2,1,0:T(2,128)(2,1)} %reshape.409), calls=%async_computation.2 | async-start | bytes 2621440 | tf_op jit(solution)/shard_map/all_to_all | solution.py:71
  276.4 1.6 copy-start.6
  278.1 4.8 %copy-start.2 = (bf16[16,2048,64]{1,2,0:T(8,128)(2,1)S(1)}, bf16[16,2048,64]{1,2,0:T(8,128)(2,1)}, u32[]{:S(2)}) copy-start(bf16[16,2048,64]{1,2,0:T(8,128)(2,1)} %copy.55) | copy-start | bytes 12582916
  285.7 1.8 copy-start.1
Sparse Core Ops, SparseCore 0:
  9.2 99.5 all-gather.6
  110.6 39.3 all-gather.8
  151.8 54.4 all-gather.10
  207.9 54.3 all-gather.12
where the time goes:
time: 295 us; the launch traced here: 294 us
  waiting for transfers between devices  141 us (48%)
  local copies, waits for them, and re-layouts  57.4 us (19%)
  other arithmetic  41.3 us (14%)
  matrix products  25.3 us (9%)
  starting transfers between devices  15.9 us (5%)
  between operations  13.4 us (5%)
    all_gather x1, waiting for transfers between devices, in_one_piece(): result = lax.all_gather(both, axis, axis=dim, tiled=True)  97.2 us
    unnamed x2, other arithmetic  28.8 us
    all_gather x2, waiting for transfers between devices, on_gathered_pieces(): blocks = [lax.all_gather(piece, axis) for piece in pieces]  25.8 us
    convert_element_type x1, local copies, waits for them, and re-layouts, body(): (opened * mixed_sum.reshape(members, seq_len, groups_dev, group_dim)).ast...  20.9 us
    all_gather x2, local copies, waits for them, and re-layouts, on_gathered_pieces(): blocks = [lax.all_gather(piece, axis) for piece in pieces]  17.3 us
    dot_general x2, matrix products, contract(): return jnp.dot(flat_rows, shard_rows, preferred_element_type=jnp.float32)  12.6 us
    all_to_all x1, waiting for transfers between devices, body(): lax.all_to_all(by_group(gate_proj), 'sp', split_axis=2, concat_axis=1, ti...  12.5 us
    unnamed x19, local copies, waits for them, and re-layouts  9.69 us
  transfers between devices with their start and end apart: 7, of which 4 were waited for; matrix products, arithmetic and copies ran while one was open for 36% of the time, Pallas kernels for 0%

commit v1 on v0

v1 whole, which is shorter than its diff:
```python
import functools

import jax
import jax.numpy as jnp
from jax import lax
from jax.experimental import pallas as pl
from jax.experimental.pallas import tpu as pltpu
from jax.sharding import PartitionSpec as P

norm_eps = 1e-06
NX, NY, NZ = 4, 4, 8
ROWS = 320
SPAN = 1280
WIDTH = 2048
GD = 128
MROWS = 80
f32 = jnp.float32
bf16 = jnp.bfloat16


def remote(src, dst, send, recv, dev):
    return pltpu.make_async_remote_copy(
        src_ref=src,
        dst_ref=dst,
        send_sem=send,
        recv_sem=recv,
        device_id=dev,
        device_id_type=pl.DeviceIdType.MESH,
    )


def gelu(a):
    return 0.5 * a * (1.0 + jnp.tanh(0.7978845608028654 * (a + 0.044715 * (a * a * a))))


def kernel(
    tokens, upw, gatew, gain, mixw, bias, ogain, outw, out_ref,
    tok, wb, mb, ob, v, op, bt, g, ab, nb, sb, sg,
    lsem, xsend, xrecv, zmsend, zmrecv, zwsend, zwrecv, zosend, zorecv,
    ysend, yrecv, bmsend, bmrecv, bwsend, bwrecv, bosend, borecv,
    asend, arecv, ssend, srecv, asem,
):
    sp = lax.axis_index("sp")
    dp = lax.axis_index("dp")
    y, x = lax.div(sp, NX), lax.rem(sp, NX)
    z, c = lax.div(dp, 2), lax.rem(dp, 2)

    def dev(xx, yy, zz, cc):
        return {"sp": yy * NX + xx, "dp": zz * 2 + cc}

    def mod(a, n):
        return lax.rem(a, n)

    nextx = dev(mod(x + 1 + 2 * c, NX), y, z, c)
    nexty = dev(x, mod(y + 1 + 2 * c, NY), z, c)
    nextz = dev(x, y, mod(z + 1 + 6 * c, NZ), c)
    sib = dev(x, y, z, 1 - c)

    def xat(h):
        return mod(x + h * (3 - 2 * c), NX)

    def yat(h, cc):
        return mod(y + h * (3 - 2 * cc), NY)

    def zat(t, cc):
        return mod(z + t * (7 - 6 * cc), NZ)

    d = z * 2 + c
    loads = [
        pltpu.make_async_copy(tokens.at[0], tok.at[x], lsem.at[0]),
        pltpu.make_async_copy(
            mixw.at[0], mb.at[y, pl.ds(pl.multiple_of(d * MROWS, 16), MROWS), :], lsem.at[1]
        ),
        pltpu.make_async_copy(
            outw, ob.at[:, pl.ds(pl.multiple_of(d * GD, GD), GD)], lsem.at[2]
        ),
        pltpu.make_async_copy(bias, sb.at[y], lsem.at[3]),
        pltpu.make_async_copy(gain, sg.at[y], lsem.at[4]),
    ]
    wrow = pl.ds(pl.multiple_of(d * GD, GD), GD)
    for j in range(4):
        cols = pl.ds(pl.multiple_of((x + 4 * j) * GD, GD), GD)
        loads.append(
            pltpu.make_async_copy(upw.at[:, cols], wb.at[wrow, pl.ds(j * GD, GD)], lsem.at[5 + j])
        )
        loads.append(
            pltpu.make_async_copy(
                gatew.at[:, cols], wb.at[wrow, pl.ds(512 + j * GD, GD)], lsem.at[9 + j]
            )
        )
    for load in loads:
        load.start()

    barrier = pltpu.get_barrier_semaphore()
    peers = [dev(mod(x + k, NX), y, z, c) for k in (1, 2, 3)]
    peers += [dev(x, mod(y + k, NY), z, c) for k in (1, 2, 3)]
    peers += [dev(x, y, mod(z + k, NZ), c) for k in (1, NZ - 1)]
    peers += [sib]
    for peer in peers:
        pl.semaphore_signal(barrier, inc=1, device_id=peer, device_id_type=pl.DeviceIdType.MESH)
    pl.semaphore_wait(barrier, len(peers))
    for load in loads:
        load.wait()

    def xcopy(i):
        hop, k = lax.div(i, 4), lax.rem(i, 4)
        slot = tok.at[xat(hop), pl.ds(pl.multiple_of(k * 80, 16), 80), :]
        return remote(slot, slot, xsend.at[i], xrecv.at[i], nextx)

    def xarrival(i):
        hop, k = lax.div(i, 4), lax.rem(i, 4)
        slot = tok.at[xat(hop + 1), pl.ds(pl.multiple_of(k * 80, 16), 80), :]
        return remote(slot, slot, xsend.at[i], xrecv.at[i], nextx)

    def xservice(i, forward):
        xarrival(i).wait_recv()
        if forward:
            xcopy(i + 4).start()

    def by_width(dd, fn):
        n = lax.div(MROWS * (dd + 1) + 255, 256)
        for k in range(1, 6):
            @pl.when(n == k)
            def _():
                fn(256 * k)

    def mslot(group, dd, width):
        return mb.at[group, pl.ds(pl.multiple_of(dd * MROWS, 16), MROWS), pl.ds(0, width)]

    def mservice(t, arrived):
        dd = zat(t, c) * 2 + c

        def go(width):
            slot = mslot(y, dd, width)
            if arrived:
                remote(slot, slot, zmsend.at[t - 1], zmrecv.at[t - 1], nextz).wait_recv()

            @pl.when(t < NZ - 1)
            def _():
                remote(slot, slot, zmsend.at[t], zmrecv.at[t], nextz).start()

            remote(slot, slot, ysend.at[t], yrecv.at[t], nexty).start()
            remote(slot, slot, bmsend.at[t], bmrecv.at[t], sib).start()

        by_width(dd, go)

    def yservice(h, s):
        dd = zat(s, c) * 2 + c

        def go(width):
            slot = mslot(yat(h + 1, c), dd, width)
            i = h * 8 + s
            remote(slot, slot, ysend.at[i], yrecv.at[i], nexty).wait_recv()
            if h < 2:
                remote(slot, slot, ysend.at[i + 8], yrecv.at[i + 8], nexty).start()
            remote(slot, slot, bmsend.at[i + 8], bmrecv.at[i + 8], sib).start()

        by_width(dd, go)

    def yround(t):
        for h in range(3):
            s = t - 1 - h

            @pl.when((s >= 0) & (s < 8))
            def _():
                yservice(h, s)

    def wslot(t, half, cc):
        dd = zat(t, cc) * 2 + cc
        return wb.at[
            pl.ds(pl.multiple_of(dd * GD, GD), GD), pl.ds(512 * half, 512)
        ]

    def wservice(t, half, arrived):
        slot = wslot(t, half, c)
        if arrived:
            i = (t - 1) * 2 + half
            remote(slot, slot, zwsend.at[i], zwrecv.at[i], nextz).wait_recv()

        @pl.when(t < NZ - 1)
        def _():
            i = t * 2 + half
            remote(slot, slot, zwsend.at[i], zwrecv.at[i], nextz).start()

        i = t * 2 + half
        remote(slot, slot, bwsend.at[i], bwrecv.at[i], sib).start()

    def oslot(t, q, cc):
        dd = zat(t, cc) * 2 + cc
        return ob.at[pl.ds(512 * q, 512), pl.ds(pl.multiple_of(dd * GD, GD), GD)]

    def ofull(t, cc):
        dd = zat(t, cc) * 2 + cc
        return ob.at[:, pl.ds(pl.multiple_of(dd * GD, GD), GD)]

    def oservice(t):
        for q in range(4):
            slot = oslot(t, q, c)
            if t > 0:
                i = (t - 1) * 4 + q
                remote(slot, slot, zosend.at[i], zorecv.at[i], nextz).wait_recv()
            if t < NZ - 1:
                i = t * 4 + q
                remote(slot, slot, zosend.at[i], zorecv.at[i], nextz).start()
        slot = ofull(t, c)
        remote(slot, slot, bosend.at[t], borecv.at[t], sib).start()

    for k in (1, 2, 3):
        peer = dev(x, mod(y + k, NY), z, c)
        remote(sb.at[y], sb.at[y], ssend.at[k - 1], srecv.at[k - 1], peer).start()
        remote(sg.at[y], sg.at[y], ssend.at[k + 2], srecv.at[k + 2], peer).start()
    mservice(0, False)
    for i in range(4):
        xcopy(i).start()
    wservice(0, 0, False)
    wservice(0, 1, False)

    def round_(t, _):
        mservice(t, True)
        yround(t)
        wservice(t, 0, True)
        xservice(t - 1, True)
        wservice(t, 1, True)

        return 0

    lax.fori_loop(1, NZ - 1, round_, 0)
    oservice(0)
    lax.fori_loop(NZ - 1, NZ, round_, 0)

    for t in range(NZ):
        for half in range(2):
            slot = wslot(t, half, 1 - c)
            remote(slot, slot, bwsend.at[2 * t + half], bwrecv.at[2 * t + half], sib).wait_recv()
    for k in (1, 2, 3):
        src = mod(y + NY - k, NY)
        peer = dev(x, src, z, c)
        remote(sb.at[src], sb.at[src], ssend.at[k - 1], srecv.at[k - 1], peer).wait_recv()
        remote(sg.at[src], sg.at[src], ssend.at[k + 2], srecv.at[k + 2], peer).wait_recv()

    def project(xs, r0, n):
        start = pl.multiple_of(xs * ROWS + r0, 16)

        def pair(jj, _):
            t = tok[xs, pl.ds(pl.multiple_of(r0, 16), n), :]
            up = jnp.dot(
                t, wb[:, pl.ds(pl.multiple_of(jj * 256, 256), 256)], preferred_element_type=f32
            )
            gate = jnp.dot(
                t,
                wb[:, pl.ds(pl.multiple_of(512 + jj * 256, 256), 256)],
                preferred_element_type=f32,
            )
            for i in range(2):
                j = 2 * jj + i
                u = up[:, i * GD:(i + 1) * GD].astype(bf16).astype(f32)
                op[j, pl.ds(start, n), :] = gelu(u)
                a = gelu(gate[:, i * GD:(i + 1) * GD].astype(bf16).astype(f32))
                a = a - jnp.mean(a, axis=-1, keepdims=True)
                spread = jnp.mean(a * a, axis=-1, keepdims=True)
                v[j, pl.ds(start, n), :] = (
                    a * lax.rsqrt(spread + norm_eps) * sg[j]
                ).astype(bf16)
            return 0

        lax.fori_loop(0, 2, pair, 0)

    def project_shard(h):
        xs = xat(h)

        def half(i, _):
            project(xs, i * 160, 160)
            return 0

        lax.fori_loop(0, 2, half, 0)

    def spread_bias(j, _):
        bt[j] = jnp.transpose(jnp.broadcast_to(sb[j], (GD, SPAN)))
        return 0

    project_shard(0)
    yround(8)
    project_shard(1)
    xservice(7, True)
    oservice(1)
    yround(9)
    project_shard(2)
    yround(10)
    lax.fori_loop(0, 4, spread_bias, 0)
    oservice(2)

    for i in range(8, 12):
        xservice(i, False)
        project(xat(3), (i - 8) * 80, 80)

    for h in range(4):
        def msib(t, _):
            dd = zat(t, 1 - c) * 2 + 1 - c

            def go(width):
                slot = mslot(yat(h, 1 - c), dd, width)
                i = h * 8 + t
                remote(slot, slot, bmsend.at[i], bmrecv.at[i], sib).wait_recv()

            by_width(dd, go)
            return 0

        lax.fori_loop(0, 8, msib, 0)

    kmax = (384, 640, 1024, 1280)
    kfree = (0, 256, 640, 896)

    def acopy(j, r):
        lanes = pl.ds(pl.multiple_of((4 * j + x) * GD, GD), GD)
        src = g.at[j, pl.ds(ROWS * r, ROWS), :]
        return remote(src, ab.at[:, lanes], asend.at[r * 4 + j], arecv.at[x * 4 + j], dev(r, y, z, c))

    def alocal(j, r):
        lanes = pl.ds(pl.multiple_of((4 * j + x) * GD, GD), GD)
        src = g.at[j, pl.ds(ROWS * r, ROWS), :]
        return pltpu.make_async_copy(src, ab.at[:, lanes], asem.at[j])

    def mix(j, _):
        for r in range(4):
            rows = pl.ds(ROWS * r, ROWS)
            k0, k1 = kfree[r], kmax[r]
            at_row = lax.broadcasted_iota(jnp.int32, (ROWS, k1 - k0), 0) + ROWS * r
            at_col = lax.broadcasted_iota(jnp.int32, (ROWS, k1 - k0), 1) + k0
            edge = mb[j, rows, k0:k1].astype(f32)
            edge = jnp.where(at_col <= at_row, edge, 0.0).astype(bf16)
            total = jnp.dot(edge, v[j, k0:k1, :], preferred_element_type=f32)
            if k0:
                total += jnp.dot(
                    mb[j, rows, 0:k0], v[j, 0:k0, :], preferred_element_type=f32
                )
            g[j, rows, :] = (op[j, rows, :] * (total + bt[j, rows, :])).astype(bf16)

            @pl.when(x != r)
            def _():
                acopy(j, r).start()

            @pl.when(x == r)
            def _():
                alocal(j, r).start()
        return 0

    lax.fori_loop(0, 4, mix, 0)
    oservice(3)
    oservice(4)

    def await_gated(j, _):
        for k in (1, 2, 3):
            src = mod(x + k, NX)
            lanes = pl.ds(pl.multiple_of((4 * j + src) * GD, GD), GD)
            slot = ab.at[:, lanes]
            remote(slot, slot, asend.at[0], arecv.at[src * 4 + j], sib).wait_recv()
        for r in range(4):
            @pl.when(x == r)
            def _():
                alocal(j, r).wait()
        return 0

    lax.fori_loop(0, 4, await_gated, 0)

    def rms(i, _):
        rows = pl.ds(pl.multiple_of(i * 16, 16), 16)
        a = ab[rows, :].astype(f32)
        scale = lax.rsqrt(jnp.mean(a * a, axis=-1, keepdims=True) + norm_eps)
        nb[rows, :] = (a * scale * ogain[...]).astype(bf16)
        return 0

    lax.fori_loop(0, ROWS // 16, rms, 0)
    oservice(5)

    def osib(t):
        slot = ofull(t, 1 - c)
        remote(slot, slot, bosend.at[t], borecv.at[t], sib).wait_recv()

    def emit(zz):
        cols = pl.ds(pl.multiple_of(zz * 256, 256), 256)
        out_ref[0, :, cols] = jnp.dot(nb[...], ob[:, cols], preferred_element_type=f32).astype(bf16)

    for t in range(6):
        osib(t)
    for k in (0, 4, 3, 5):
        emit(mod(z + k, NZ))
    for t in (6, 7):
        oservice(t)
        osib(t)
        emit(mod(z + 8 - t, NZ))
        emit(mod(z + t, NZ))

    for k in (1, 2, 3):
        remote(sb.at[y], sb.at[y], ssend.at[k - 1], srecv.at[k - 1], sib).wait_send()
        remote(sg.at[y], sg.at[y], ssend.at[k + 2], srecv.at[k + 2], sib).wait_send()

    def xsent(i, _):
        xcopy(i).wait_send()
        return 0

    lax.fori_loop(0, 12, xsent, 0)

    def msent(t, _):
        dd = zat(t, c) * 2 + c

        def go(width):
            slot = mslot(y, dd, width)

            @pl.when(t < NZ - 1)
            def _():
                remote(slot, slot, zmsend.at[t], zmrecv.at[t], nextz).wait_send()

            for h in range(4):
                i = h * 8 + t
                if h < 3:
                    remote(slot, slot, ysend.at[i], yrecv.at[i], nexty).wait_send()
                remote(slot, slot, bmsend.at[i], bmrecv.at[i], sib).wait_send()

        by_width(dd, go)

        for half in range(2):
            slot = wslot(t, half, c)
            i = t * 2 + half

            @pl.when(t < NZ - 1)
            def _():
                remote(slot, slot, zwsend.at[i], zwrecv.at[i], nextz).wait_send()

            remote(slot, slot, bwsend.at[i], bwrecv.at[i], sib).wait_send()

        @pl.when(t < NZ - 1)
        def _():
            for q in range(4):
                slot = oslot(t, q, c)
                remote(slot, slot, zosend.at[t * 4 + q], zorecv.at[t * 4 + q], nextz).wait_send()

        slot = ofull(t, c)
        remote(slot, slot, bosend.at[t], borecv.at[t], sib).wait_send()
        return 0

    lax.fori_loop(0, 8, msent, 0)

    def asent(j, _):
        for r in range(4):
            @pl.when(x != r)
            def _():
                acopy(j, r).wait_send()
        return 0

    lax.fori_loop(0, 4, asent, 0)


def body(tokens, up_weight, gate_weight, group_gain, mix_weight, mix_bias, out_gain, out_weight):
    hbm = pl.BlockSpec(memory_space=pl.ANY)
    vmem = pl.BlockSpec(memory_space=pltpu.VMEM)
    dma = pltpu.SemaphoreType.DMA
    return pl.pallas_call(
        kernel,
        out_shape=jax.ShapeDtypeStruct((1, ROWS, WIDTH), bf16),
        in_specs=[hbm, hbm, hbm, hbm, hbm, hbm, vmem, hbm],
        out_specs=vmem,
        scratch_shapes=[
            pltpu.VMEM((NX, ROWS, WIDTH), bf16),
            pltpu.VMEM((WIDTH, 1024), bf16),
            pltpu.VMEM((4, SPAN, SPAN), bf16),
            pltpu.VMEM((WIDTH, WIDTH), bf16),
            pltpu.VMEM((4, SPAN, GD), bf16),
            pltpu.VMEM((4, SPAN, GD), f32),
            pltpu.VMEM((4, SPAN, GD), f32),
            pltpu.VMEM((4, SPAN, GD), bf16),
            pltpu.VMEM((ROWS, WIDTH), bf16),
            pltpu.VMEM((ROWS, WIDTH), bf16),
            pltpu.VMEM((4, 1, SPAN), f32),
            pltpu.VMEM((4, 1, GD), f32),
            dma((13,)),
            dma((12,)), dma((12,)),
            dma((7,)), dma((7,)),
            dma((14,)), dma((14,)),
            dma((28,)), dma((28,)),
            dma((24,)), dma((24,)),
            dma((32,)), dma((32,)),
            dma((16,)), dma((16,)),
            dma((8,)), dma((8,)),
            dma((16,)), dma((16,)),
            dma((6,)), dma((6,)),
            dma((4,)),
        ],
        compiler_params=pltpu.CompilerParams(
            collective_id=0, has_side_effects=True, vmem_limit_bytes=66_000_000
        ),
        name="gating",
    )(
        tokens, up_weight, gate_weight, group_gain, mix_weight, mix_bias,
        out_gain.reshape(1, WIDTH), out_weight,
    )


def solution(mesh):
    return jax.shard_map(
        body,
        mesh=mesh,
        in_specs=(
            P("dp", "sp", None),
            P("dp", None),
            P("dp", None),
            P("sp", None),
            P("sp", "dp", None),
            P("sp", None),
            P(),
            P(None, "dp"),
        ),
        out_specs=P("dp", "sp", None),
        check_vma=False,
    )
```

time: 295 us -> 113 us (0.38)
  waiting for transfers between devices: 141 us -> 0 us
  Pallas kernels: 0 us -> 110 us
  local copies, waits for them, and re-layouts: 57.4 us -> 2.52 us
  other arithmetic: 41.3 us -> 0 us
  matrix products: 25.3 us -> 0 us
  starting transfers between devices: 15.9 us -> 0 us
  between operations: 13.4 us -> 0.01 us
    all_gather x4 -> x0, waiting for transfers between devices: 123 us -> none  [the longest x1 97.2 us: in_one_piece(): result = lax.all_gather(both, axis, axis=dim, tiled=True)]
    pallas_call x0 -> x1, Pallas kernels: none -> 110 us  [body(): pl.pallas_call(kernel, out_shape=jax.ShapeDtypeStruct((1, ROWS, WIDTH), b...]
    unnamed x2 -> x0, other arithmetic: 28.8 us -> none
    convert_element_type x3 -> x0, local copies, waits for them, and re-layouts: 24 us -> none  [the longest x1 20.9 us: body(): (opened * mixed_sum.reshape(members, seq_len, groups_dev, group_dim)).ast...]
    dot_general x3 -> x0, matrix products: 18 us -> none  [the longest x2 12.6 us: contract(): return jnp.dot(flat_rows, shard_rows, preferred_element_type=jnp.float32)]
    all_gather x2 -> x0, local copies, waits for them, and re-layouts: 17.3 us -> none  [on_gathered_pieces(): blocks = [lax.all_gather(piece, axis) for piece in pieces]]
    all_to_all x3 -> x0, waiting for transfers between devices: 16.4 us -> none  [the longest x1 12.5 us: body(): lax.all_to_all(by_group(gate_proj), 'sp', split_axis=2, concat_axis=1, ti...]
    all_to_all x3 -> x0, starting transfers between devices: 15.8 us -> none  [the longest x1 6.53 us: body(): lax.all_to_all(by_group(gate_proj), 'sp', split_axis=2, concat_axis=1, ti...]
  transfers between devices with their start and end apart: 7 -> 0, of which waited for: 4 -> 0; matrix products, arithmetic and copies ran while one was open for 36% -> 0% of each run, Pallas kernels for 0% -> 0%
where the time goes in v1:
time: 113 us
  Pallas kernels  110 us (97%)
  local copies, waits for them, and re-layouts  2.52 us (2%)
    pallas_call x1, Pallas kernels, body(): pl.pallas_call(kernel, out_shape=jax.ShapeDtypeStruct((1, ROWS, WIDTH), b...  110 us
    unnamed x1, local copies, waits for them, and re-layouts  2.52 us

profile of v1, /device:TPU:1, one launch (start us, length us, event | category | flops | bytes accessed | tf_op | source)
XLA Modules:
  0.0 113.0 jit_solution(9740193145533438748)
XLA Ops:
  0.0 110.5 %gating.1 = bf16[1,320,2048]{2,1,0:T(8,128)(2,1)} custom-call(bf16[1,320,2048]{2,1,0:T(8,128)(2,1)} %tokens.1, bf16[128,2048]{1,0:T(8,128)(2,1)} %upw.1, bf16[128,2048]{1,0:T(8,128)(2,1)} %gatew.1, f32[1,128]{1,0:T(1,128)} %gain.1, bf16[1,80,1280]{2,1,0:T(8,128)(2,1)} %mixw.1, f32[1,1280]{1,0:T(1,128)} %bias.1, f32[1,2048]{1,0:T(1,128)} %bitcast.1, ...), custom_call_target="tpu_custom_call" | custom-call | tf_op jit(solution)/shard_map/gating/pallas_call | solution.py:457
  110.5 2.5 %copy.10 = bf16[1,320,2048]{2,1,0:T(8,128)(2,1)} copy(bf16[1,320,2048]{2,1,0:T(8,128)(2,1)} %gating.1) | data formatting | bytes 2621440

commit v2 on v0

v2 whole, which is shorter than its diff:
```python
import functools

import jax
import jax.numpy as jnp
from jax import lax
from jax.experimental import pallas as pl
from jax.experimental.pallas import tpu as pltpu
from jax.sharding import PartitionSpec as P

norm_eps = 1e-06
NX, NY, NZ = 4, 4, 8
ROWS = 320
SPAN = 1280
WIDTH = 2048
GD = 128
MROWS = 80
OZ = 1024
OQ = (WIDTH - OZ) // 4
XN = 4
XR = ROWS // XN
MSUM = (352, 384)
f32 = jnp.float32
bf16 = jnp.bfloat16


def remote(src, dst, send, recv, dev):
    return pltpu.make_async_remote_copy(
        src_ref=src,
        dst_ref=dst,
        send_sem=send,
        recv_sem=recv,
        device_id=dev,
        device_id_type=pl.DeviceIdType.MESH,
    )


def gelu(a):
    return 0.5 * a * (1.0 + jnp.tanh(0.7978845608028654 * (a + 0.044715 * (a * a * a))))


def kernel(
    tokens, upw, gatew, gain, mixw, bias, ogain, outw, out_ref,
    tok, wb, mb, ob, v, op, bt, g, ab, nb, sb, sg,
    lsem, xsend, xrecv, zmsend, zmrecv, zwsend, zwrecv, zqsend, zqrecv,
    zpsend, zprecv, ysend, yrecv, oysend, oyrecv, bsend, brecv,
    asend, arecv, ssend, srecv, asem,
):
    sp = lax.axis_index("sp")
    dp = lax.axis_index("dp")
    y, x = lax.div(sp, NX), lax.rem(sp, NX)
    z, c = lax.div(dp, 2), lax.rem(dp, 2)

    def dev(xx, yy, zz, cc):
        return {"sp": yy * NX + xx, "dp": zz * 2 + cc}

    def mod(a, n):
        return lax.rem(a, n)

    tox = [dev(mod(x + 1, NX), y, z, c), dev(mod(x + NX - 1, NX), y, z, c)]
    toy = [dev(x, mod(y + 1, NY), z, c), dev(x, mod(y + NY - 1, NY), z, c)]
    toz = [dev(x, y, mod(z + 1, NZ), c), dev(x, y, mod(z + NZ - 1, NZ), c)]
    sib = dev(x, y, z, 1 - c)

    def xorg(r, way):
        return mod(x + (NX - r if way == 0 else r), NX)

    def yorg(r, way):
        return mod(y + (NY - r if way == 0 else r), NY)

    def zorg(r, way):
        return mod(z + (NZ - r if way == 0 else r), NZ)

    d = z * 2 + c
    wrow = pl.ds(pl.multiple_of(d * GD, GD), GD)
    loads = [
        pltpu.make_async_copy(
            mixw.at[0], mb.at[y, pl.ds(pl.multiple_of(d * MROWS, 16), MROWS), :], lsem.at[1]
        ),
        pltpu.make_async_copy(tokens.at[0], tok.at[x], lsem.at[0]),
        pltpu.make_async_copy(outw, ob.at[:, wrow], lsem.at[2]),
        pltpu.make_async_copy(bias, sb.at[y], lsem.at[3]),
        pltpu.make_async_copy(gain, sg.at[y], lsem.at[4]),
    ]
    for load in loads:
        load.start()
    for j in range(4):
        cols = pl.ds(pl.multiple_of((x + 4 * j) * GD, GD), GD)
        for half, w in enumerate((upw, gatew)):
            pltpu.make_async_copy(
                w.at[:, cols], wb.at[wrow, pl.ds(512 * half + j * GD, GD)], lsem.at[5]
            ).start()
    loads.append(pltpu.make_async_copy(wb.at[wrow, :], wb.at[wrow, :], lsem.at[5]))

    barrier = pltpu.get_barrier_semaphore()
    peers = [dev(mod(x + k, NX), y, z, c) for k in (1, 2, 3)]
    peers += [dev(x, mod(y + k, NY), z, c) for k in (1, 2, 3)]
    peers += toz + [sib]
    for peer in peers:
        pl.semaphore_signal(barrier, inc=1, device_id=peer, device_id_type=pl.DeviceIdType.MESH)
    pl.semaphore_wait(barrier, len(peers))
    for load in loads:
        load.wait()

    def xslot(shard, k):
        return tok.at[shard, pl.ds(k * XR, XR), :]

    xfrom1 = mod(x + NX - 1 + 2 * c, NX)
    xfrom2 = mod(x + 2, NX)
    xto = dev(mod(x + 1 + 2 * c, NX), y, z, c)

    def xforward(k):
        slot = xslot(xfrom1, k)
        remote(slot, slot, xsend.at[0], xrecv.at[c * XN + k], xto).wait_recv()
        remote(slot, slot, xsend.at[0], xrecv.at[2 * XN + k], xto).start()

    def by_width(dd, fn):
        n = lax.div(MROWS * (dd + 1) + GD - 1, GD)
        for k in range(1, 11):
            @pl.when(n == k)
            def _():
                fn(GD * k)

    def mslot(group, dd, width):
        return mb.at[group, pl.ds(pl.multiple_of(dd * MROWS, 16), MROWS), pl.ds(0, width)]

    def steps(r, way):
        if r == 0:
            return z, None, [0, 1], 0
        if r == 4:
            return mod(z + 4, NZ), 6 + c, [], 7
        return zorg(r, way), (r - 1) * 2 + way, [way], 2 * r - 1 + way

    def onward(r, way, start):
        for w in way:
            if r < 3:
                start(w)
            else:
                @pl.when(c == w)
                def _():
                    start(w)

    def mstep(r, way=None):
        org, at, ways, k = steps(r, way)
        dd = org * 2 + c

        def go(width):
            slot = mslot(y, dd, width)
            if at is not None:
                remote(slot, slot, zmsend.at[0], zmrecv.at[at], sib).wait_recv()

            def start(w):
                i = r * 2 + w
                remote(slot, slot, zmsend.at[i], zmrecv.at[i], toz[w]).start()

            onward(r, ways, start)
            for w in range(2):
                remote(slot, slot, ysend.at[0], yrecv.at[w * 8 + k], toy[w]).start()
            remote(slot, slot, bsend.at[0], brecv.at[0], sib).start()

        by_width(dd, go)

    def ygroup(a):
        return mod(y + 2, NY) if a == 2 else yorg(1, a)

    def kchip(k):
        if k == 0:
            return z
        if k == 7:
            return mod(z + 4, NZ)
        return zorg((k + 1) // 2, (k + 1) % 2)

    def ystep(a, k):
        dd = kchip(k) * 2 + c

        def go(width):
            slot = mslot(ygroup(a), dd, width)
            remote(slot, slot, ysend.at[0], yrecv.at[a * 8 + k], sib).wait_recv()
            if a < 2:
                @pl.when(c == a)
                def _():
                    remote(slot, slot, ysend.at[0], yrecv.at[16 + k], toy[a]).start()
            remote(slot, slot, bsend.at[0], brecv.at[0], sib).start()

        by_width(dd, go)

    def wstep(r, half, way=None):
        org, at, ways, k = steps(r, way)
        slot = wb.at[
            pl.ds(pl.multiple_of((org * 2 + c) * GD, GD), GD), pl.ds(512 * half, 512)
        ]
        if at is not None:
            remote(slot, slot, zwsend.at[0], zwrecv.at[at * 2 + half], sib).wait_recv()

        def start(w):
            i = (r * 2 + w) * 2 + half
            remote(slot, slot, zwsend.at[0], zwrecv.at[i], toz[w]).start()

        onward(r, ways, start)
        remote(slot, slot, bsend.at[1], brecv.at[1], sib).start()

    def qstep(r, half, way=None):
        org, at, ways, k = steps(r, way)
        slot = ob.at[
            pl.ds(OZ // 2 * half, OZ // 2), pl.ds(pl.multiple_of((org * 2 + c) * GD, GD), GD)
        ]
        if at is not None:
            remote(slot, slot, zqsend.at[0], zqrecv.at[at * 2 + half], sib).wait_recv()

        def start(w):
            i = (r * 2 + w) * 2 + half
            remote(slot, slot, zqsend.at[0], zqrecv.at[i], toz[w]).start()

        onward(r, ways, start)
        remote(slot, slot, bsend.at[2], brecv.at[2], sib).start()

    def pslot(group, chip):
        rows = pl.ds(pl.multiple_of(OZ + OQ * group, 16), OQ)
        return ob.at[rows, pl.ds(pl.multiple_of((chip * 2 + c) * GD, GD), GD)]

    def pstep(r, way=None):
        org, at, ways, k = steps(r, way)
        slot = pslot(y, org)
        if at is not None:
            remote(slot, slot, zpsend.at[0], zprecv.at[at], sib).wait_recv()

        def start(w):
            i = r * 2 + w
            remote(slot, slot, zpsend.at[0], zprecv.at[i], toz[w]).start()

        onward(r, ways, start)
        for w in range(2):
            remote(slot, slot, oysend.at[0], oyrecv.at[w * 8 + k], toy[w]).start()
        remote(slot, slot, bsend.at[3], brecv.at[3], sib).start()

    def pystep(a, k):
        slot = pslot(ygroup(a), kchip(k))
        remote(slot, slot, oysend.at[0], oyrecv.at[a * 8 + k], sib).wait_recv()
        if a < 2:
            @pl.when(c == a)
            def _():
                remote(slot, slot, oysend.at[0], oyrecv.at[16 + k], toy[a]).start()
        remote(slot, slot, bsend.at[3], brecv.at[3], sib).start()

    def yrun(fn, ks, ways):
        for k in ks:
            for a in ways:
                fn(a, k)

    def mpair(r):
        mstep(r, 0)
        mstep(r, 1)

    def wpair(r):
        for half in range(2):
            wstep(r, half, 0)
            wstep(r, half, 1)

    def qpair(r):
        for half in range(2):
            qstep(r, half, 0)
            qstep(r, half, 1)

    def ppair(r):
        pstep(r, 0)
        pstep(r, 1)

    mstep(0)
    for k in range(XN):
        for w in range(2):
            remote(xslot(x, k), xslot(x, k), xsend.at[0], xrecv.at[w * XN + k], tox[w]).start()
    wstep(0, 0)
    wstep(0, 1)
    for k in (1, 2, 3):
        peer = dev(x, mod(y + k, NY), z, c)
        remote(sb.at[y], sb.at[y], ssend.at[0], srecv.at[0], peer).start()
        remote(sg.at[y], sg.at[y], ssend.at[1], srecv.at[1], peer).start()

    mpair(1)
    wpair(1)
    mpair(2)
    yrun(ystep, (0,), (0, 1, 2))
    wpair(2)
    xforward(0)
    yrun(ystep, (1, 2), (0, 1))
    mpair(3)
    yrun(ystep, (1, 2), (2,))
    xforward(1)
    yrun(ystep, (3, 4), (0, 1))
    wpair(3)
    pstep(0)
    qstep(0, 0)
    qstep(0, 1)
    xforward(2)
    mstep(4)
    yrun(ystep, (3, 4), (2,))
    yrun(ystep, (5, 6), (0, 1))
    wstep(4, 0)
    wstep(4, 1)
    xforward(3)
    ppair(1)

    def wait_all(ref, i):
        remote(ref, ref, bsend.at[i], brecv.at[i], sib).wait_recv()

    wait_all(wb.at[0:1024, :], 1)
    remote(sb.at[0:3], sb.at[0:3], ssend.at[0], srecv.at[0], sib).wait_recv()
    remote(sg.at[0:3], sg.at[0:3], ssend.at[1], srecv.at[1], sib).wait_recv()

    def project(xs):
        start = pl.multiple_of(xs * ROWS, 16)
        n = ROWS

        def pair(jj, _):
            t = tok[xs]
            up = jnp.dot(
                t, wb[:, pl.ds(pl.multiple_of(jj * 256, 256), 256)], preferred_element_type=f32
            )
            gate = jnp.dot(
                t,
                wb[:, pl.ds(pl.multiple_of(512 + jj * 256, 256), 256)],
                preferred_element_type=f32,
            )
            for i in range(2):
                j = 2 * jj + i
                u = up[:, i * GD:(i + 1) * GD].astype(bf16).astype(f32)
                op[j, pl.ds(start, n), :] = gelu(u)
                a = gelu(gate[:, i * GD:(i + 1) * GD].astype(bf16).astype(f32))
                a = a - jnp.mean(a, axis=-1, keepdims=True)
                spread = jnp.mean(a * a, axis=-1, keepdims=True)
                v[j, pl.ds(start, n), :] = (
                    a * lax.rsqrt(spread + norm_eps) * sg[j]
                ).astype(bf16)
            return 0

        lax.fori_loop(0, 2, pair, 0)

    def spread_bias(j, _):
        bt[j] = jnp.transpose(jnp.broadcast_to(sb[j], (GD, SPAN)))
        return 0

    project(x)
    yrun(ystep, (5, 6), (2,))
    yrun(ystep, (7,), (0, 1))
    for k in range(XN):
        slot = xslot(mod(x + 1 + 2 * c, NX), k)
        remote(slot, slot, xsend.at[0], xrecv.at[(1 - c) * XN + k], sib).wait_recv()
    project(xfrom1)
    yrun(ystep, (7,), (2,))
    yrun(pystep, (0,), (0, 1))
    qpair(1)
    project(mod(x + 1 + 2 * c, NX))
    yrun(pystep, (0,), (2,))
    yrun(pystep, (1, 2), (0, 1))
    ppair(2)
    lax.fori_loop(0, 4, spread_bias, 0)
    for k in range(XN):
        slot = xslot(xfrom2, k)
        remote(slot, slot, xsend.at[0], xrecv.at[2 * XN + k], sib).wait_recv()
    project(xfrom2)
    yrun(pystep, (1, 2), (2,))
    yrun(pystep, (3, 4), (0, 1))
    qpair(2)

    for cc in range(2):
        @pl.when(c != cc)
        def _():
            wait_all(mb.at[:, 0:MSUM[cc], :], 0)

    kmax = (384, 640, 1024, 1280)
    kfree = (0, 256, 640, 896)

    def lanes(j, xx):
        return pl.ds(pl.multiple_of((4 * j + xx) * GD, GD), GD)

    def acopy(j, r):
        src = g.at[j, pl.ds(ROWS * r, ROWS), :]
        return remote(src, ab.at[:, lanes(j, x)], asend.at[0], arecv.at[j], dev(r, y, z, c))

    def alocal(j, r):
        src = g.at[j, pl.ds(ROWS * r, ROWS), :]
        return pltpu.make_async_copy(src, ab.at[:, lanes(j, x)], asem.at[0])

    def mix(j, _):
        for r in range(4):
            rows = pl.ds(ROWS * r, ROWS)
            k0, k1 = kfree[r], kmax[r]
            at_row = lax.broadcasted_iota(jnp.int32, (ROWS, k1 - k0), 0) + ROWS * r
            at_col = lax.broadcasted_iota(jnp.int32, (ROWS, k1 - k0), 1) + k0
            edge = mb[j, rows, k0:k1].astype(f32)
            edge = jnp.where(at_col <= at_row, edge, 0.0).astype(bf16)
            total = jnp.dot(edge, v[j, k0:k1, :], preferred_element_type=f32)
            if k0:
                total += jnp.dot(
                    mb[j, rows, 0:k0], v[j, 0:k0, :], preferred_element_type=f32
                )
            g[j, rows, :] = (op[j, rows, :] * (total + bt[j, rows, :])).astype(bf16)

        for r in range(4):
            @pl.when(x != r)
            def _():
                acopy(j, r).start()

            @pl.when(x == r)
            def _():
                alocal(j, r).start()
        return 0

    lax.fori_loop(0, 2, mix, 0)
    ppair(3)
    lax.fori_loop(2, 4, mix, 0)
    yrun(pystep, (3, 4), (2,))
    yrun(pystep, (5, 6), (0, 1))
    qpair(3)
    pstep(4)
    yrun(pystep, (5, 6), (2,))
    yrun(pystep, (7,), (0, 1))
    qstep(4, 0)
    qstep(4, 1)
    yrun(pystep, (7,), (2,))

    for j in range(4):
        slot = ab.at[:, 0:3 * GD]
        remote(slot, slot, asend.at[0], arecv.at[j], sib).wait_recv()
    pltpu.make_async_copy(ab.at[:, 0:4 * GD], ab.at[:, 0:4 * GD], asem.at[0]).wait()

    def rms(i, _):
        rows = pl.ds(pl.multiple_of(i * 64, 16), 64)
        a = ab[rows, :].astype(f32)
        scale = lax.rsqrt(jnp.mean(a * a, axis=-1, keepdims=True) + norm_eps)
        nb[rows, :] = (a * scale * ogain[...]).astype(bf16)
        return 0

    lax.fori_loop(0, ROWS // 64, rms, 0)
    wait_all(ob.at[0:OZ, 0:1024], 2)
    wait_all(ob.at[0:WIDTH - OZ, 0:1024], 3)

    def emit(i, _):
        cols = pl.ds(pl.multiple_of(i * 1024, 1024), 1024)
        out_ref[0, :, cols] = jnp.dot(nb[...], ob[:, cols], preferred_element_type=f32).astype(bf16)
        return 0

    lax.fori_loop(0, 2, emit, 0)

    def sent(ref, sem):
        remote(ref, ref, sem, brecv.at[0], sib).wait_send()

    sent(sb.at[0:3], ssend.at[0])
    sent(sg.at[0:3], ssend.at[1])
    sent(tok.at[0:3], xsend.at[0])
    sent(wb.at[0:896, :], zwsend.at[0])
    sent(ob.at[0:OZ, 0:896], zqsend.at[0])
    sent(ob.at[0:OQ, 0:896], zpsend.at[0])
    sent(ob.at[0:OQ * 2, 0:1536], oysend.at[0])
    sent(wb.at[0:1024, :], bsend.at[1])
    sent(ob.at[0:OZ, 0:1024], bsend.at[2])
    sent(ob.at[0:WIDTH - OZ, 0:1024], bsend.at[3])
    sent(ab.at[:, 0:12 * GD], asend.at[0])
    for cc in range(2):
        @pl.when(c == cc)
        def _():
            sent(mb.at[:, 0:MSUM[cc], :], bsend.at[0])
            sent(mb.at[0:3, 0:MSUM[cc], :], ysend.at[0])

    def msent(i, _):
        r, w = lax.div(i, 2), lax.rem(i, 2)
        org = mod(z + lax.select(w == 0, NZ - r, r), NZ)

        def go(width):
            slot = mslot(y, org * 2 + c, width)
            remote(slot, slot, zmsend.at[i], zmrecv.at[0], sib).wait_send()

        @pl.when((i < 6) | (w == c))
        def _():
            by_width(org * 2 + c, go)
        return 0

    lax.fori_loop(0, 8, msent, 0)


def body(tokens, up_weight, gate_weight, group_gain, mix_weight, mix_bias, out_gain, out_weight):
    hbm = pl.BlockSpec(memory_space=pl.ANY)
    vmem = pl.BlockSpec(memory_space=pltpu.VMEM)
    dma = pltpu.SemaphoreType.DMA
    return pl.pallas_call(
        kernel,
        out_shape=jax.ShapeDtypeStruct((1, ROWS, WIDTH), bf16),
        in_specs=[hbm, hbm, hbm, hbm, hbm, hbm, vmem, hbm],
        out_specs=vmem,
        scratch_shapes=[
            pltpu.VMEM((NX, ROWS, WIDTH), bf16),
            pltpu.VMEM((WIDTH, 1024), bf16),
            pltpu.VMEM((4, SPAN, SPAN), bf16),
            pltpu.VMEM((WIDTH, WIDTH), bf16),
            pltpu.VMEM((4, SPAN, GD), bf16),
            pltpu.VMEM((4, SPAN, GD), f32),
            pltpu.VMEM((4, SPAN, GD), f32),
            pltpu.VMEM((4, SPAN, GD), bf16),
            pltpu.VMEM((ROWS, WIDTH), bf16),
            pltpu.VMEM((ROWS, WIDTH), bf16),
            pltpu.VMEM((4, 1, SPAN), f32),
            pltpu.VMEM((4, 1, GD), f32),
            dma((6,)),
            dma((1,)),
            dma((12,)),
            dma((8,)),
            dma((8,)),
            dma((1,)),
            dma((16,)),
            dma((1,)),
            dma((16,)),
            dma((1,)),
            dma((8,)),
            dma((1,)),
            dma((24,)),
            dma((1,)),
            dma((24,)),
            dma((4,)),
            dma((4,)),
            dma((1,)),
            dma((4,)),
            dma((2,)),
            dma((2,)),
            dma((1,)),
        ],
        compiler_params=pltpu.CompilerParams(
            collective_id=0, has_side_effects=True, vmem_limit_bytes=66_000_000
        ),
        name="gating",
    )(
        tokens, up_weight, gate_weight, group_gain, mix_weight, mix_bias,
        out_gain.reshape(1, WIDTH), out_weight,
    )


def solution(mesh):
    return jax.shard_map(
        body,
        mesh=mesh,
        in_specs=(
            P("dp", "sp", None),
            P("dp", None),
            P("dp", None),
            P("sp", None),
            P("sp", "dp", None),
            P("sp", None),
            P(),
            P(None, "dp"),
        ),
        out_specs=P("dp", "sp", None),
        check_vma=False,
    )
```

time: 295 us -> 93.5 us (0.32)
  waiting for transfers between devices: 141 us -> 0 us
  Pallas kernels: 0 us -> 90 us
  local copies, waits for them, and re-layouts: 57.4 us -> 2.52 us
  other arithmetic: 41.3 us -> 0 us
  matrix products: 25.3 us -> 0 us
  starting transfers between devices: 15.9 us -> 0 us
  between operations: 13.4 us -> 0.01 us
    all_gather x4 -> x0, waiting for transfers between devices: 123 us -> none  [the longest x1 97.2 us: in_one_piece(): result = lax.all_gather(both, axis, axis=dim, tiled=True)]
    pallas_call x0 -> x1, Pallas kernels: none -> 90 us  [body(): pl.pallas_call(kernel, out_shape=jax.ShapeDtypeStruct((1, ROWS, WIDTH), b...]
    unnamed x2 -> x0, other arithmetic: 28.8 us -> none
    convert_element_type x3 -> x0, local copies, waits for them, and re-layouts: 24 us -> none  [the longest x1 20.9 us: body(): (opened * mixed_sum.reshape(members, seq_len, groups_dev, group_dim)).ast...]
    dot_general x3 -> x0, matrix products: 18 us -> none  [the longest x2 12.6 us: contract(): return jnp.dot(flat_rows, shard_rows, preferred_element_type=jnp.float32)]
    all_gather x2 -> x0, local copies, waits for them, and re-layouts: 17.3 us -> none  [on_gathered_pieces(): blocks = [lax.all_gather(piece, axis) for piece in pieces]]
    all_to_all x3 -> x0, waiting for transfers between devices: 16.4 us -> none  [the longest x1 12.5 us: body(): lax.all_to_all(by_group(gate_proj), 'sp', split_axis=2, concat_axis=1, ti...]
    all_to_all x3 -> x0, starting transfers between devices: 15.8 us -> none  [the longest x1 6.53 us: body(): lax.all_to_all(by_group(gate_proj), 'sp', split_axis=2, concat_axis=1, ti...]
  transfers between devices with their start and end apart: 7 -> 0, of which waited for: 4 -> 0; matrix products, arithmetic and copies ran while one was open for 36% -> 0% of each run, Pallas kernels for 0% -> 0%
where the time goes in v2:
time: 93.5 us; the launch traced here: 92.5 us
  Pallas kernels  90 us (96%)
  local copies, waits for them, and re-layouts  2.52 us (3%)
    pallas_call x1, Pallas kernels, body(): pl.pallas_call(kernel, out_shape=jax.ShapeDtypeStruct((1, ROWS, WIDTH), b...  90 us
    unnamed x1, local copies, waits for them, and re-layouts  2.52 us

profile of v2, /device:TPU:1, one launch (start us, length us, event | category | flops | bytes accessed | tf_op | source)
XLA Modules:
  0.0 92.5 jit_solution(7173135007084549007)
XLA Ops:
  0.0 90.0 %gating.1 = bf16[1,320,2048]{2,1,0:T(8,128)(2,1)} custom-call(bf16[1,320,2048]{2,1,0:T(8,128)(2,1)} %tokens.1, bf16[128,2048]{1,0:T(8,128)(2,1)} %upw.1, bf16[128,2048]{1,0:T(8,128)(2,1)} %gatew.1, f32[1,128]{1,0:T(1,128)} %gain.1, bf16[1,80,1280]{2,1,0:T(8,128)(2,1)} %mixw.1, f32[1,1280]{1,0:T(1,128)} %bias.1, f32[1,2048]{1,0:T(1,128)} %bitcast.1, ...), custom_call_target="tpu_custom_call" | custom-call | tf_op jit(solution)/shard_map/gating/pallas_call | solution.py:484
  90.0 2.5 %copy.10 = bf16[1,320,2048]{2,1,0:T(8,128)(2,1)} copy(bf16[1,320,2048]{2,1,0:T(8,128)(2,1)} %gating.1) | data formatting | bytes 2621440

commit v3 on v2

--- a/solution.py
+++ b/solution.py
@@ -43,7 +43,7 @@
     tok, wb, mb, ob, v, op, bt, g, ab, nb, sb, sg,
     lsem, xsend, xrecv, zmsend, zmrecv, zwsend, zwrecv, zqsend, zqrecv,
     zpsend, zprecv, ysend, yrecv, oysend, oyrecv, bsend, brecv,
-    asend, arecv, ssend, srecv, asem,
+    asend, arecv, ssend, srecv, asem, osem, ov, og,
 ):
     sp = lax.axis_index("sp")
     dp = lax.axis_index("dp")
@@ -80,6 +80,7 @@
         pltpu.make_async_copy(outw, ob.at[:, wrow], lsem.at[2]),
         pltpu.make_async_copy(bias, sb.at[y], lsem.at[3]),
         pltpu.make_async_copy(gain, sg.at[y], lsem.at[4]),
+        pltpu.make_async_copy(ogain, og, lsem.at[6]),
     ]
     for load in loads:
         load.start()
@@ -276,27 +277,28 @@
         remote(sg.at[y], sg.at[y], ssend.at[1], srecv.at[1], peer).start()
 
     mpair(1)
+    yrun(ystep, (0,), (0, 1))
     wpair(1)
     mpair(2)
-    yrun(ystep, (0,), (0, 1, 2))
+    yrun(ystep, (1, 2), (0, 1))
+    xforward(0)
     wpair(2)
-    xforward(0)
-    yrun(ystep, (1, 2), (0, 1))
+    yrun(ystep, (0,), (2,))
     mpair(3)
-    yrun(ystep, (1, 2), (2,))
     xforward(1)
     yrun(ystep, (3, 4), (0, 1))
     wpair(3)
     pstep(0)
     qstep(0, 0)
     qstep(0, 1)
+    mstep(4)
     xforward(2)
-    mstep(4)
-    yrun(ystep, (3, 4), (2,))
     yrun(ystep, (5, 6), (0, 1))
+    yrun(ystep, (1, 2), (2,))
     wstep(4, 0)
     wstep(4, 1)
     xforward(3)
+    yrun(ystep, (7,), (0, 1))
     ppair(1)
 
     def wait_all(ref, i):
@@ -339,27 +341,24 @@
         return 0
 
     project(x)
-    yrun(ystep, (5, 6), (2,))
-    yrun(ystep, (7,), (0, 1))
+    yrun(pystep, (0,), (0, 1))
+    yrun(ystep, (3, 4), (2,))
     for k in range(XN):
         slot = xslot(mod(x + 1 + 2 * c, NX), k)
         remote(slot, slot, xsend.at[0], xrecv.at[(1 - c) * XN + k], sib).wait_recv()
     project(xfrom1)
+    qpair(1)
+    yrun(ystep, (5, 6), (2,))
+    project(mod(x + 1 + 2 * c, NX))
+    ppair(2)
+    yrun(pystep, (1, 2), (0, 1))
+    lax.fori_loop(0, 4, spread_bias, 0)
     yrun(ystep, (7,), (2,))
-    yrun(pystep, (0,), (0, 1))
-    qpair(1)
-    project(mod(x + 1 + 2 * c, NX))
-    yrun(pystep, (0,), (2,))
-    yrun(pystep, (1, 2), (0, 1))
-    ppair(2)
-    lax.fori_loop(0, 4, spread_bias, 0)
     for k in range(XN):
         slot = xslot(xfrom2, k)
         remote(slot, slot, xsend.at[0], xrecv.at[2 * XN + k], sib).wait_recv()
     project(xfrom2)
-    yrun(pystep, (1, 2), (2,))
-    yrun(pystep, (3, 4), (0, 1))
-    qpair(2)
+    yrun(pystep, (0,), (2,))
 
     for cc in range(2):
         @pl.when(c != cc)
@@ -406,17 +405,23 @@
         return 0
 
     lax.fori_loop(0, 2, mix, 0)
+    yrun(pystep, (3, 4), (0, 1))
+    lax.fori_loop(2, 4, mix, 0)
     ppair(3)
-    lax.fori_loop(2, 4, mix, 0)
+    qpair(2)
+    yrun(pystep, (1, 2), (2,))
     yrun(pystep, (3, 4), (2,))
+    pstep(4)
+    qstep(3, 0, 0)
+    qstep(3, 0, 1)
     yrun(pystep, (5, 6), (0, 1))
-    qpair(3)
-    pstep(4)
+    qstep(3, 1, 0)
+    qstep(3, 1, 1)
+    yrun(pystep, (7,), (0, 1))
     yrun(pystep, (5, 6), (2,))
-    yrun(pystep, (7,), (0, 1))
     qstep(4, 0)
+    yrun(pystep, (7,), (2,))
     qstep(4, 1)
-    yrun(pystep, (7,), (2,))
 
     for j in range(4):
         slot = ab.at[:, 0:3 * GD]
@@ -427,7 +432,7 @@
         rows = pl.ds(pl.multiple_of(i * 64, 16), 64)
         a = ab[rows, :].astype(f32)
         scale = lax.rsqrt(jnp.mean(a * a, axis=-1, keepdims=True) + norm_eps)
-        nb[rows, :] = (a * scale * ogain[...]).astype(bf16)
+        nb[rows, :] = (a * scale * og[...]).astype(bf16)
         return 0
 
     lax.fori_loop(0, ROWS // 64, rms, 0)
@@ -436,7 +441,8 @@
 
     def emit(i, _):
         cols = pl.ds(pl.multiple_of(i * 1024, 1024), 1024)
-        out_ref[0, :, cols] = jnp.dot(nb[...], ob[:, cols], preferred_element_type=f32).astype(bf16)
+        ov[:, cols] = jnp.dot(nb[...], ob[:, cols], preferred_element_type=f32).astype(bf16)
+        pltpu.make_async_copy(ov.at[:, cols], out_ref.at[0, :, cols], osem.at[0]).start()
         return 0
 
     lax.fori_loop(0, 2, emit, 0)
@@ -475,17 +481,17 @@
         return 0
 
     lax.fori_loop(0, 8, msent, 0)
+    pltpu.make_async_copy(ov, out_ref.at[0], osem.at[0]).wait()
 
 
 def body(tokens, up_weight, gate_weight, group_gain, mix_weight, mix_bias, out_gain, out_weight):
-    hbm = pl.BlockSpec(memory_space=pl.ANY)
-    vmem = pl.BlockSpec(memory_space=pltpu.VMEM)
+    hbm = pl.BlockSpec(memory_space=pltpu.HBM)
     dma = pltpu.SemaphoreType.DMA
     return pl.pallas_call(
         kernel,
         out_shape=jax.ShapeDtypeStruct((1, ROWS, WIDTH), bf16),
-        in_specs=[hbm, hbm, hbm, hbm, hbm, hbm, vmem, hbm],
-        out_specs=vmem,
+        in_specs=[hbm] * 8,
+        out_specs=pl.BlockSpec(memory_space=pl.ANY),
         scratch_shapes=[
             pltpu.VMEM((NX, ROWS, WIDTH), bf16),
             pltpu.VMEM((WIDTH, 1024), bf16),
@@ -499,7 +505,7 @@
             pltpu.VMEM((ROWS, WIDTH), bf16),
             pltpu.VMEM((4, 1, SPAN), f32),
             pltpu.VMEM((4, 1, GD), f32),
-            dma((6,)),
+            dma((7,)),
             dma((1,)),
             dma((12,)),
             dma((8,)),
@@ -521,14 +527,22 @@
             dma((2,)),
             dma((2,)),
             dma((1,)),
+            dma((1,)),
+            pltpu.VMEM((ROWS, WIDTH), bf16),
+            pltpu.VMEM((1, WIDTH), f32),
         ],
         compiler_params=pltpu.CompilerParams(
-            collective_id=0, has_side_effects=True, vmem_limit_bytes=66_000_000
+            collective_id=0, has_side_effects=True, vmem_limit_bytes=46_000_000
         ),
         name="gating",
     )(
-        tokens, up_weight, gate_weight, group_gain, mix_weight, mix_bias,
-        out_gain.reshape(1, WIDTH), out_weight,
+        *(
+            pltpu.with_memory_space_constraint(a, pltpu.HBM)
+            for a in (
+                tokens, up_weight, gate_weight, group_gain, mix_weight, mix_bias,
+                out_gain.reshape(1, WIDTH), out_weight,
+            )
+        )
     )
 
 

time: 93.5 us -> 85.1 us (0.910)
  Pallas kernels: 90 us -> 84 us
  local copies, waits for them, and re-layouts: 2.52 us -> 1.06 us
    pallas_call x1, Pallas kernels: 90 us -> 84 us  [body(): pl.pallas_call(kernel, out_shape=jax.ShapeDtypeStruct((1, ROWS, WIDTH), b...]
    unnamed x1, local copies, waits for them, and re-layouts: 2.52 us -> 1.06 us
where the time goes in v3:
time: 85.1 us; the launch traced here: 85 us
  Pallas kernels  84 us (99%)
  local copies, waits for them, and re-layouts  1.06 us (1%)
    pallas_call x1, Pallas kernels, body(): pl.pallas_call(kernel, out_shape=jax.ShapeDtypeStruct((1, ROWS, WIDTH), b...  84 us

profile of v3, /device:TPU:1, one launch (start us, length us, event | category | flops | bytes accessed | tf_op | source)
XLA Modules:
  0.0 85.0 jit_solution(15627460905766402310)
XLA Ops:
  0.0 84.0 %gating.1 = bf16[1,320,2048]{2,1,0:T(8,128)(2,1)S(1)} custom-call(bf16[1,320,2048]{2,1,0:T(8,128)(2,1)} %tokens.1, bf16[128,2048]{1,0:T(8,128)(2,1)} %upw.1, bf16[128,2048]{1,0:T(8,128)(2,1)} %gatew.1, f32[1,128]{1,0:T(1,128)} %gain.1, bf16[1,80,1280]{2,1,0:T(8,128)(2,1)} %mixw.1, f32[1,1280]{1,0:T(1,128)} %bias.1, f32[1,2048]{1,0:T(1,128)} %bitcast.1, ...), custom_call_target="tpu_custom_call" | custom-call | tf_op jit(solution)/shard_map/gating/pallas_call | solution.py:490
  84.0 1.1 %copy.10 = bf16[1,320,2048]{2,1,0:T(8,128)(2,1)} copy(bf16[1,320,2048]{2,1,0:T(8,128)(2,1)S(1)} %gating.1) | data formatting | bytes 2621440

commit v4 on v3

--- a/solution.py
+++ b/solution.py
@@ -14,7 +14,7 @@
 WIDTH = 2048
 GD = 128
 MROWS = 80
-OZ = 1024
+OZ = 768
 OQ = (WIDTH - OZ) // 4
 XN = 4
 XR = ROWS // XN
@@ -43,7 +43,7 @@
     tok, wb, mb, ob, v, op, bt, g, ab, nb, sb, sg,
     lsem, xsend, xrecv, zmsend, zmrecv, zwsend, zwrecv, zqsend, zqrecv,
     zpsend, zprecv, ysend, yrecv, oysend, oyrecv, bsend, brecv,
-    asend, arecv, ssend, srecv, asem, osem, ov, og,
+    asend, arecv, ssend, srecv, asem, osem, ov, og, acc, ss, pa,
 ):
     sp = lax.axis_index("sp")
     dp = lax.axis_index("dp")
@@ -124,24 +124,32 @@
     def mslot(group, dd, width):
         return mb.at[group, pl.ds(pl.multiple_of(dd * MROWS, 16), MROWS), pl.ds(0, width)]
 
+    def last_way(chip):
+        return lax.div(mod(chip + 6, NZ), 4)
+
+    light = [last_way(mod(z + 1, NZ)) == 0, last_way(mod(z + NZ - 1, NZ)) == 1]
+    alternate = [c == 0, c == 1]
+
     def steps(r, way):
         if r == 0:
             return z, None, [0, 1], 0
         if r == 4:
-            return mod(z + 4, NZ), 6 + c, [], 7
+            return mod(z + 4, NZ), 6, [], 7
         return zorg(r, way), (r - 1) * 2 + way, [way], 2 * r - 1 + way
 
-    def onward(r, way, start):
+    def onward(r, way, start, last):
         for w in way:
             if r < 3:
                 start(w)
             else:
-                @pl.when(c == w)
+                @pl.when(last[w])
                 def _():
                     start(w)
 
     def mstep(r, way=None):
         org, at, ways, k = steps(r, way)
+        if r == 4:
+            at = at + last_way(z)
         dd = org * 2 + c
 
         def go(width):
@@ -153,7 +161,7 @@
                 i = r * 2 + w
                 remote(slot, slot, zmsend.at[i], zmrecv.at[i], toz[w]).start()
 
-            onward(r, ways, start)
+            onward(r, ways, start, light)
             for w in range(2):
                 remote(slot, slot, ysend.at[0], yrecv.at[w * 8 + k], toy[w]).start()
             remote(slot, slot, bsend.at[0], brecv.at[0], sib).start()
@@ -186,6 +194,8 @@
 
     def wstep(r, half, way=None):
         org, at, ways, k = steps(r, way)
+        if r == 4:
+            at = at + last_way(z)
         slot = wb.at[
             pl.ds(pl.multiple_of((org * 2 + c) * GD, GD), GD), pl.ds(512 * half, 512)
         ]
@@ -194,13 +204,15 @@
 
         def start(w):
             i = (r * 2 + w) * 2 + half
-            remote(slot, slot, zwsend.at[0], zwrecv.at[i], toz[w]).start()
-
-        onward(r, ways, start)
-        remote(slot, slot, bsend.at[1], brecv.at[1], sib).start()
+            remote(slot, slot, zwsend.at[0 if r < 3 else 1 + w], zwrecv.at[i], toz[w]).start()
+
+        onward(r, ways, start, light)
+        remote(slot, slot, bsend.at[1], brecv.at[1 if r < 3 else 4], sib).start()
 
     def qstep(r, half, way=None):
         org, at, ways, k = steps(r, way)
+        if r == 4:
+            at = at + c
         slot = ob.at[
             pl.ds(OZ // 2 * half, OZ // 2), pl.ds(pl.multiple_of((org * 2 + c) * GD, GD), GD)
         ]
@@ -211,7 +223,7 @@
             i = (r * 2 + w) * 2 + half
             remote(slot, slot, zqsend.at[0], zqrecv.at[i], toz[w]).start()
 
-        onward(r, ways, start)
+        onward(r, ways, start, alternate)
         remote(slot, slot, bsend.at[2], brecv.at[2], sib).start()
 
     def pslot(group, chip):
@@ -220,6 +232,8 @@
 
     def pstep(r, way=None):
         org, at, ways, k = steps(r, way)
+        if r == 4:
+            at = at + c
         slot = pslot(y, org)
         if at is not None:
             remote(slot, slot, zpsend.at[0], zprecv.at[at], sib).wait_recv()
@@ -228,7 +242,7 @@
             i = r * 2 + w
             remote(slot, slot, zpsend.at[0], zprecv.at[i], toz[w]).start()
 
-        onward(r, ways, start)
+        onward(r, ways, start, alternate)
         for w in range(2):
             remote(slot, slot, oysend.at[0], oyrecv.at[w * 8 + k], toy[w]).start()
         remote(slot, slot, bsend.at[3], brecv.at[3], sib).start()
@@ -264,6 +278,68 @@
     def ppair(r):
         pstep(r, 0)
         pstep(r, 1)
+
+    def spread_bias(j, _):
+        bt[j] = jnp.transpose(jnp.broadcast_to(sb[j], (GD, SPAN)))
+        return 0
+
+    def activate(up, gate, jj, start, n):
+        for i in range(2):
+            j = 2 * jj + i
+            u = up[:, i * GD:(i + 1) * GD].astype(bf16).astype(f32)
+            op[j, pl.ds(start, n), :] = gelu(u)
+            a = gelu(gate[:, i * GD:(i + 1) * GD].astype(bf16).astype(f32))
+            a = a - jnp.mean(a, axis=-1, keepdims=True)
+            spread = jnp.mean(a * a, axis=-1, keepdims=True)
+            v[j, pl.ds(start, n), :] = (a * lax.rsqrt(spread + norm_eps) * sg[j]).astype(bf16)
+
+    def wcols(half, jj):
+        return pl.ds(pl.multiple_of(512 * half + jj * 256, 256), 256)
+
+    def project(xs, row=0, n=ROWS, pairs=(0, 2)):
+        start = pl.multiple_of(xs * ROWS + row, 16)
+
+        def pair(jj, _):
+            t = tok[xs, row:row + n, :]
+            up = jnp.dot(t, wb[:, wcols(0, jj)], preferred_element_type=f32)
+            gate = jnp.dot(t, wb[:, wcols(1, jj)], preferred_element_type=f32)
+            activate(up, gate, jj, start, n)
+            return 0
+
+        lax.fori_loop(*pairs, pair, 0)
+
+    def over_chips(xs, chips, half, jj):
+        total = None
+        for chip in chips:
+            rows = pl.ds(pl.multiple_of(chip * 256, 256), 256)
+            p = jnp.dot(tok[xs, :, rows], wb[rows, wcols(half, jj)], preferred_element_type=f32)
+            total = p if total is None else total + p
+        return total
+
+    near = [z] + [zorg(r, w) for r in (1, 2) for w in range(2)]
+    far = [zorg(3, 0), zorg(3, 1), mod(z + 4, NZ)]
+
+    def project_near(xs, i):
+        def tile(k, _):
+            half, jj = lax.div(k, 2), lax.rem(k, 2)
+            pa[i, :, wcols(half, jj)] = over_chips(xs, near, half, jj)
+            return 0
+
+        lax.fori_loop(0, 4, tile, 0)
+
+    def project_far(xs, i):
+        start = pl.multiple_of(xs * ROWS, 16)
+
+        def pair(jj, _):
+            up = pa[i, :, wcols(0, jj)] + over_chips(xs, far, 0, jj)
+            gate = pa[i, :, wcols(1, jj)] + over_chips(xs, far, 1, jj)
+            activate(up, gate, jj, start, ROWS)
+            return 0
+
+        lax.fori_loop(0, 2, pair, 0)
+
+    def wait_all(ref, i):
+        remote(ref, ref, bsend.at[i], brecv.at[i], sib).wait_recv()
 
     mstep(0)
     for k in range(XN):
@@ -282,11 +358,16 @@
     mpair(2)
     yrun(ystep, (1, 2), (0, 1))
     xforward(0)
+    remote(sb.at[0:3], sb.at[0:3], ssend.at[0], srecv.at[0], sib).wait_recv()
+    remote(sg.at[0:3], sg.at[0:3], ssend.at[1], srecv.at[1], sib).wait_recv()
+    lax.fori_loop(0, 4, spread_bias, 0)
     wpair(2)
     yrun(ystep, (0,), (2,))
     mpair(3)
     xforward(1)
     yrun(ystep, (3, 4), (0, 1))
+    wait_all(wb.at[0:640, :], 1)
+    project_near(x, 0)
     wpair(3)
     pstep(0)
     qstep(0, 0)
@@ -295,75 +376,45 @@
     xforward(2)
     yrun(ystep, (5, 6), (0, 1))
     yrun(ystep, (1, 2), (2,))
+    xforward(3)
+    project_near(xfrom1, 1)
     wstep(4, 0)
     wstep(4, 1)
-    xforward(3)
+
+
+    xother = mod(x + 1 + 2 * c, NX)
+    for k in range(XN):
+        slot = xslot(xother, k)
+        remote(slot, slot, xsend.at[0], xrecv.at[(1 - c) * XN + k], sib).wait_recv()
+    project_near(xother, 2)
+    wait_all(wb.at[0:384, :], 4)
+    project_far(x, 0)
     yrun(ystep, (7,), (0, 1))
     ppair(1)
-
-    def wait_all(ref, i):
-        remote(ref, ref, bsend.at[i], brecv.at[i], sib).wait_recv()
-
-    wait_all(wb.at[0:1024, :], 1)
-    remote(sb.at[0:3], sb.at[0:3], ssend.at[0], srecv.at[0], sib).wait_recv()
-    remote(sg.at[0:3], sg.at[0:3], ssend.at[1], srecv.at[1], sib).wait_recv()
-
-    def project(xs):
-        start = pl.multiple_of(xs * ROWS, 16)
-        n = ROWS
-
-        def pair(jj, _):
-            t = tok[xs]
-            up = jnp.dot(
-                t, wb[:, pl.ds(pl.multiple_of(jj * 256, 256), 256)], preferred_element_type=f32
-            )
-            gate = jnp.dot(
-                t,
-                wb[:, pl.ds(pl.multiple_of(512 + jj * 256, 256), 256)],
-                preferred_element_type=f32,
-            )
-            for i in range(2):
-                j = 2 * jj + i
-                u = up[:, i * GD:(i + 1) * GD].astype(bf16).astype(f32)
-                op[j, pl.ds(start, n), :] = gelu(u)
-                a = gelu(gate[:, i * GD:(i + 1) * GD].astype(bf16).astype(f32))
-                a = a - jnp.mean(a, axis=-1, keepdims=True)
-                spread = jnp.mean(a * a, axis=-1, keepdims=True)
-                v[j, pl.ds(start, n), :] = (
-                    a * lax.rsqrt(spread + norm_eps) * sg[j]
-                ).astype(bf16)
-            return 0
-
-        lax.fori_loop(0, 2, pair, 0)
-
-    def spread_bias(j, _):
-        bt[j] = jnp.transpose(jnp.broadcast_to(sb[j], (GD, SPAN)))
-        return 0
-
-    project(x)
     yrun(pystep, (0,), (0, 1))
     yrun(ystep, (3, 4), (2,))
-    for k in range(XN):
-        slot = xslot(mod(x + 1 + 2 * c, NX), k)
-        remote(slot, slot, xsend.at[0], xrecv.at[(1 - c) * XN + k], sib).wait_recv()
-    project(xfrom1)
+    project_far(xfrom1, 1)
     qpair(1)
     yrun(ystep, (5, 6), (2,))
-    project(mod(x + 1 + 2 * c, NX))
-    ppair(2)
-    yrun(pystep, (1, 2), (0, 1))
-    lax.fori_loop(0, 4, spread_bias, 0)
-    yrun(ystep, (7,), (2,))
-    for k in range(XN):
+    project_far(xother, 2)
+
+    def xlast(k):
         slot = xslot(xfrom2, k)
         remote(slot, slot, xsend.at[0], xrecv.at[2 * XN + k], sib).wait_recv()
-    project(xfrom2)
-    yrun(pystep, (0,), (2,))
+
+    for k in range(XN - 1):
+        xlast(k)
+    project(xfrom2, 0, ROWS - XR)
+    ppair(2)
+    yrun(ystep, (7,), (2,))
 
     for cc in range(2):
         @pl.when(c != cc)
         def _():
             wait_all(mb.at[:, 0:MSUM[cc], :], 0)
+
+    xlast(XN - 1)
+    project(xfrom2, ROWS - XR, XR, (0, 1))
 
     kmax = (384, 640, 1024, 1280)
     kfree = (0, 256, 640, 896)
@@ -404,48 +455,73 @@
                 alocal(j, r).start()
         return 0
 
-    lax.fori_loop(0, 2, mix, 0)
-    yrun(pystep, (3, 4), (0, 1))
-    lax.fori_loop(2, 4, mix, 0)
+    lax.fori_loop(0, 1, mix, 0)
+    yrun(pystep, (1, 2), (0, 1))
+    lax.fori_loop(1, 2, mix, 0)
     ppair(3)
     qpair(2)
-    yrun(pystep, (1, 2), (2,))
-    yrun(pystep, (3, 4), (2,))
+    project(xfrom2, ROWS - XR, XR, (1, 2))
+    lax.fori_loop(2, 3, mix, 0)
+    yrun(pystep, (3, 4), (0, 1))
+    lax.fori_loop(3, 4, mix, 0)
     pstep(4)
     qstep(3, 0, 0)
     qstep(3, 0, 1)
     yrun(pystep, (5, 6), (0, 1))
     qstep(3, 1, 0)
     qstep(3, 1, 1)
+    yrun(pystep, (0, 1, 2), (2,))
     yrun(pystep, (7,), (0, 1))
+    yrun(pystep, (3, 4), (2,))
+    qstep(4, 0)
+    qstep(4, 1)
     yrun(pystep, (5, 6), (2,))
-    qstep(4, 0)
-    yrun(pystep, (7,), (2,))
-    qstep(4, 1)
-
-    for j in range(4):
+
+    pltpu.make_async_copy(ab.at[:, 0:4 * GD], ab.at[:, 0:4 * GD], asem.at[0]).wait()
+
+    def partial_out(j):
         slot = ab.at[:, 0:3 * GD]
         remote(slot, slot, asend.at[0], arecv.at[j], sib).wait_recv()
-    pltpu.make_async_copy(ab.at[:, 0:4 * GD], ab.at[:, 0:4 * GD], asem.at[0]).wait()
-
-    def rms(i, _):
-        rows = pl.ds(pl.multiple_of(i * 64, 16), 64)
-        a = ab[rows, :].astype(f32)
-        scale = lax.rsqrt(jnp.mean(a * a, axis=-1, keepdims=True) + norm_eps)
-        nb[rows, :] = (a * scale * og[...]).astype(bf16)
-        return 0
-
-    lax.fori_loop(0, ROWS // 64, rms, 0)
+        k0 = 512 * j
+
+        def prepare(i, _):
+            rows = pl.ds(pl.multiple_of(i * 64, 16), 64)
+            squares = jnp.zeros((64, GD), f32)
+            for k in range(k0, k0 + 512, GD):
+                a = ab[rows, k:k + GD].astype(f32)
+                squares += a * a
+                nb[rows, k:k + GD] = (a * og[:, k:k + GD]).astype(bf16)
+            if j:
+                squares += ss[rows, :]
+            ss[rows, :] = squares
+            return 0
+
+        lax.fori_loop(0, ROWS // 64, prepare, 0)
+        if j == 3:
+            mean = jnp.sum(ss[...], axis=-1, keepdims=True) * (1.0 / WIDTH)
+            scale = lax.rsqrt(mean + norm_eps)
+
+        def product(i, _):
+            cols = pl.ds(pl.multiple_of(i * 1024, 1024), 1024)
+            p = jnp.dot(nb[:, k0:k0 + 512], ob[k0:k0 + 512, cols], preferred_element_type=f32)
+            if j:
+                p += acc[:, cols]
+            if j < 3:
+                acc[:, cols] = p
+            else:
+                ov[:, cols] = (p * scale).astype(bf16)
+                pltpu.make_async_copy(ov.at[:, cols], out_ref.at[0, :, cols], osem.at[0]).start()
+            return 0
+
+        lax.fori_loop(0, 2, product, 0)
+
     wait_all(ob.at[0:OZ, 0:1024], 2)
+    partial_out(0)
+    yrun(pystep, (7,), (2,))
     wait_all(ob.at[0:WIDTH - OZ, 0:1024], 3)
-
-    def emit(i, _):
-        cols = pl.ds(pl.multiple_of(i * 1024, 1024), 1024)
-        ov[:, cols] = jnp.dot(nb[...], ob[:, cols], preferred_element_type=f32).astype(bf16)
-        pltpu.make_async_copy(ov.at[:, cols], out_ref.at[0, :, cols], osem.at[0]).start()
-        return 0
-
-    lax.fori_loop(0, 2, emit, 0)
+    partial_out(1)
+    partial_out(2)
+    partial_out(3)
 
     def sent(ref, sem):
         remote(ref, ref, sem, brecv.at[0], sib).wait_send()
@@ -453,7 +529,11 @@
     sent(sb.at[0:3], ssend.at[0])
     sent(sg.at[0:3], ssend.at[1])
     sent(tok.at[0:3], xsend.at[0])
-    sent(wb.at[0:896, :], zwsend.at[0])
+    sent(wb.at[0:768, :], zwsend.at[0])
+    for w in range(2):
+        @pl.when(light[w])
+        def _():
+            sent(wb.at[0:GD, :], zwsend.at[1 + w])
     sent(ob.at[0:OZ, 0:896], zqsend.at[0])
     sent(ob.at[0:OQ, 0:896], zpsend.at[0])
     sent(ob.at[0:OQ * 2, 0:1536], oysend.at[0])
@@ -475,7 +555,7 @@
             slot = mslot(y, org * 2 + c, width)
             remote(slot, slot, zmsend.at[i], zmrecv.at[0], sib).wait_send()
 
-        @pl.when((i < 6) | (w == c))
+        @pl.when((i < 6) | ((i == 6) & light[0]) | ((i == 7) & light[1]))
         def _():
             by_width(org * 2 + c, go)
         return 0
@@ -510,7 +590,7 @@
             dma((12,)),
             dma((8,)),
             dma((8,)),
-            dma((1,)),
+            dma((3,)),
             dma((16,)),
             dma((1,)),
             dma((16,)),
@@ -521,7 +601,7 @@
             dma((1,)),
             dma((24,)),
             dma((4,)),
-            dma((4,)),
+            dma((5,)),
             dma((1,)),
             dma((4,)),
             dma((2,)),
@@ -530,9 +610,12 @@
             dma((1,)),
             pltpu.VMEM((ROWS, WIDTH), bf16),
             pltpu.VMEM((1, WIDTH), f32),
+            pltpu.VMEM((ROWS, WIDTH), f32),
+            pltpu.VMEM((ROWS, GD), f32),
+            pltpu.VMEM((3, ROWS, 1024), f32),
         ],
         compiler_params=pltpu.CompilerParams(
-            collective_id=0, has_side_effects=True, vmem_limit_bytes=46_000_000
+            collective_id=0, has_side_effects=True, vmem_limit_bytes=54_000_000
         ),
         name="gating",
     )(

time: 85.1 us -> 81.3 us (0.955)
  Pallas kernels: 84 us -> 80.2 us
    pallas_call x1, Pallas kernels: 84 us -> 80.2 us  [body(): pl.pallas_call(kernel, out_shape=jax.ShapeDtypeStruct((1, ROWS, WIDTH), b...]
where the time goes in v4:
time: 81.3 us; the launch traced here: 81.2 us
  Pallas kernels  80.2 us (99%)
  local copies, waits for them, and re-layouts  1.06 us (1%)
    pallas_call x1, Pallas kernels, body(): pl.pallas_call(kernel, out_shape=jax.ShapeDtypeStruct((1, ROWS, WIDTH), b...  80.2 us

profile of v4, /device:TPU:1, one launch (start us, length us, event | category | flops | bytes accessed | tf_op | source)
XLA Modules:
  0.0 81.2 jit_solution(4401072090949707157)
XLA Ops:
  0.0 80.2 %gating.1 = bf16[1,320,2048]{2,1,0:T(8,128)(2,1)S(1)} custom-call(bf16[1,320,2048]{2,1,0:T(8,128)(2,1)} %tokens.1, bf16[128,2048]{1,0:T(8,128)(2,1)} %upw.1, bf16[128,2048]{1,0:T(8,128)(2,1)} %gatew.1, f32[1,128]{1,0:T(1,128)} %gain.1, bf16[1,80,1280]{2,1,0:T(8,128)(2,1)} %mixw.1, f32[1,1280]{1,0:T(1,128)} %bias.1, f32[1,2048]{1,0:T(1,128)} %bitcast.1, ...), custom_call_target="tpu_custom_call" | custom-call | tf_op jit(solution)/shard_map/gating/pallas_call | solution.py:570
  80.2 1.1 %copy.10 = bf16[1,320,2048]{2,1,0:T(8,128)(2,1)} copy(bf16[1,320,2048]{2,1,0:T(8,128)(2,1)S(1)} %gating.1) | data formatting | bytes 2621440

commit v5 on v4

--- a/solution.py
+++ b/solution.py
@@ -14,7 +14,8 @@
 WIDTH = 2048
 GD = 128
 MROWS = 80
-OZ = 768
+OZ = 896
+KA = min(OZ, 1024) // 256 * 256
 OQ = (WIDTH - OZ) // 4
 XN = 4
 XR = ROWS // XN
@@ -404,17 +405,18 @@
 
     for k in range(XN - 1):
         xlast(k)
-    project(xfrom2, 0, ROWS - XR)
+    project(xfrom2, 0, ROWS - XR, (0, 1))
     ppair(2)
     yrun(ystep, (7,), (2,))
+    project(xfrom2, 0, ROWS - XR, (1, 2))
+
+    xlast(XN - 1)
+    project(xfrom2, ROWS - XR, XR, (0, 1))
 
     for cc in range(2):
         @pl.when(c != cc)
         def _():
             wait_all(mb.at[:, 0:MSUM[cc], :], 0)
-
-    xlast(XN - 1)
-    project(xfrom2, ROWS - XR, XR, (0, 1))
 
     kmax = (384, 640, 1024, 1280)
     kfree = (0, 256, 640, 896)
@@ -458,10 +460,13 @@
     lax.fori_loop(0, 1, mix, 0)
     yrun(pystep, (1, 2), (0, 1))
     lax.fori_loop(1, 2, mix, 0)
-    ppair(3)
-    qpair(2)
+    qstep(2, 0, 0)
+    qstep(2, 0, 1)
     project(xfrom2, ROWS - XR, XR, (1, 2))
     lax.fori_loop(2, 3, mix, 0)
+    ppair(3)
+    qstep(2, 1, 0)
+    qstep(2, 1, 1)
     yrun(pystep, (3, 4), (0, 1))
     lax.fori_loop(3, 4, mix, 0)
     pstep(4)
@@ -479,15 +484,14 @@
 
     pltpu.make_async_copy(ab.at[:, 0:4 * GD], ab.at[:, 0:4 * GD], asem.at[0]).wait()
 
-    def partial_out(j):
+    def prepare(j):
         slot = ab.at[:, 0:3 * GD]
         remote(slot, slot, asend.at[0], arecv.at[j], sib).wait_recv()
-        k0 = 512 * j
-
-        def prepare(i, _):
+
+        def piece(i, _):
             rows = pl.ds(pl.multiple_of(i * 64, 16), 64)
             squares = jnp.zeros((64, GD), f32)
-            for k in range(k0, k0 + 512, GD):
+            for k in range(512 * j, 512 * j + 512, GD):
                 a = ab[rows, k:k + GD].astype(f32)
                 squares += a * a
                 nb[rows, k:k + GD] = (a * og[:, k:k + GD]).astype(bf16)
@@ -496,17 +500,19 @@
             ss[rows, :] = squares
             return 0
 
-        lax.fori_loop(0, ROWS // 64, prepare, 0)
-        if j == 3:
+        lax.fori_loop(0, ROWS // 64, piece, 0)
+
+    def partial_out(k0, k1):
+        if k1 == WIDTH:
             mean = jnp.sum(ss[...], axis=-1, keepdims=True) * (1.0 / WIDTH)
             scale = lax.rsqrt(mean + norm_eps)
 
         def product(i, _):
             cols = pl.ds(pl.multiple_of(i * 1024, 1024), 1024)
-            p = jnp.dot(nb[:, k0:k0 + 512], ob[k0:k0 + 512, cols], preferred_element_type=f32)
-            if j:
+            p = jnp.dot(nb[:, k0:k1], ob[k0:k1, cols], preferred_element_type=f32)
+            if k0:
                 p += acc[:, cols]
-            if j < 3:
+            if k1 < WIDTH:
                 acc[:, cols] = p
             else:
                 ov[:, cols] = (p * scale).astype(bf16)
@@ -515,13 +521,30 @@
 
         lax.fori_loop(0, 2, product, 0)
 
+    def msent(i, _):
+        r, w = lax.div(i, 2), lax.rem(i, 2)
+        org = mod(z + lax.select(w == 0, NZ - r, r), NZ)
+
+        def go(width):
+            slot = mslot(y, org * 2 + c, width)
+            remote(slot, slot, zmsend.at[i], zmrecv.at[0], sib).wait_send()
+
+        @pl.when((i < 6) | ((i == 6) & light[0]) | ((i == 7) & light[1]))
+        def _():
+            by_width(org * 2 + c, go)
+        return 0
+
+    lax.fori_loop(0, 8, msent, 0)
+    prepare(0)
+    prepare(1)
     wait_all(ob.at[0:OZ, 0:1024], 2)
-    partial_out(0)
     yrun(pystep, (7,), (2,))
+    partial_out(0, KA)
+    prepare(2)
     wait_all(ob.at[0:WIDTH - OZ, 0:1024], 3)
-    partial_out(1)
-    partial_out(2)
-    partial_out(3)
+    partial_out(KA, 1536)
+    prepare(3)
+    partial_out(1536, WIDTH)
 
     def sent(ref, sem):
         remote(ref, ref, sem, brecv.at[0], sib).wait_send()
@@ -547,20 +570,6 @@
             sent(mb.at[:, 0:MSUM[cc], :], bsend.at[0])
             sent(mb.at[0:3, 0:MSUM[cc], :], ysend.at[0])
 
-    def msent(i, _):
-        r, w = lax.div(i, 2), lax.rem(i, 2)
-        org = mod(z + lax.select(w == 0, NZ - r, r), NZ)
-
-        def go(width):
-            slot = mslot(y, org * 2 + c, width)
-            remote(slot, slot, zmsend.at[i], zmrecv.at[0], sib).wait_send()
-
-        @pl.when((i < 6) | ((i == 6) & light[0]) | ((i == 7) & light[1]))
-        def _():
-            by_width(org * 2 + c, go)
-        return 0
-
-    lax.fori_loop(0, 8, msent, 0)
     pltpu.make_async_copy(ov, out_ref.at[0], osem.at[0]).wait()
 
 

time: 81.3 us -> 79.1 us (0.973)
  Pallas kernels: 80.2 us -> 78 us
    pallas_call x1, Pallas kernels: 80.2 us -> 78 us  [body(): pl.pallas_call(kernel, out_shape=jax.ShapeDtypeStruct((1, ROWS, WIDTH), b...]
where the time goes in v5:
time: 79.1 us; the launch traced here: 79 us
  Pallas kernels  78 us (99%)
  local copies, waits for them, and re-layouts  1.06 us (1%)
    pallas_call x1, Pallas kernels, body(): pl.pallas_call(kernel, out_shape=jax.ShapeDtypeStruct((1, ROWS, WIDTH), b...  78 us

profile of v5, /device:TPU:1, one launch (start us, length us, event | category | flops | bytes accessed | tf_op | source)
XLA Modules:
  0.0 79.0 jit_solution(7740559886287425572)
XLA Ops:
  0.0 78.0 %gating.1 = bf16[1,320,2048]{2,1,0:T(8,128)(2,1)S(1)} custom-call(bf16[1,320,2048]{2,1,0:T(8,128)(2,1)} %tokens.1, bf16[128,2048]{1,0:T(8,128)(2,1)} %upw.1, bf16[128,2048]{1,0:T(8,128)(2,1)} %gatew.1, f32[1,128]{1,0:T(1,128)} %gain.1, bf16[1,80,1280]{2,1,0:T(8,128)(2,1)} %mixw.1, f32[1,1280]{1,0:T(1,128)} %bias.1, f32[1,2048]{1,0:T(1,128)} %bitcast.1, ...), custom_call_target="tpu_custom_call" | custom-call | tf_op jit(solution)/shard_map/gating/pallas_call | solution.py:579
  78.0 1.1 %copy.10 = bf16[1,320,2048]{2,1,0:T(8,128)(2,1)} copy(bf16[1,320,2048]{2,1,0:T(8,128)(2,1)S(1)} %gating.1) | data formatting | bytes 2621440

commit v6 on v5

--- a/solution.py
+++ b/solution.py
@@ -14,7 +14,7 @@
 WIDTH = 2048
 GD = 128
 MROWS = 80
-OZ = 896
+OZ = 832
 KA = min(OZ, 1024) // 256 * 256
 OQ = (WIDTH - OZ) // 4
 XN = 4
@@ -472,13 +472,13 @@
     pstep(4)
     qstep(3, 0, 0)
     qstep(3, 0, 1)
-    yrun(pystep, (5, 6), (0, 1))
     qstep(3, 1, 0)
     qstep(3, 1, 1)
+    yrun(pystep, (5, 6), (0, 1))
     yrun(pystep, (0, 1, 2), (2,))
     yrun(pystep, (7,), (0, 1))
+    qstep(4, 0)
     yrun(pystep, (3, 4), (2,))
-    qstep(4, 0)
     qstep(4, 1)
     yrun(pystep, (5, 6), (2,))
 

time: 79.1 us -> 78.7 us (level)
  no operation moved by 1% of the time
where the time goes in v6:
time: 78.7 us; the launch traced here: 78.6 us
  Pallas kernels  77.5 us (98%)
  local copies, waits for them, and re-layouts  1.06 us (1%)
    pallas_call x1, Pallas kernels, body(): pl.pallas_call(kernel, out_shape=jax.ShapeDtypeStruct((1, ROWS, WIDTH), b...  77.5 us

profile of v6, /device:TPU:1, one launch (start us, length us, event | category | flops | bytes accessed | tf_op | source)
XLA Modules:
  0.0 78.6 jit_solution(3363376281555978935)
XLA Ops:
  0.0 77.5 %gating.1 = bf16[1,320,2048]{2,1,0:T(8,128)(2,1)S(1)} custom-call(bf16[1,320,2048]{2,1,0:T(8,128)(2,1)} %tokens.1, bf16[128,2048]{1,0:T(8,128)(2,1)} %upw.1, bf16[128,2048]{1,0:T(8,128)(2,1)} %gatew.1, f32[1,128]{1,0:T(1,128)} %gain.1, bf16[1,80,1280]{2,1,0:T(8,128)(2,1)} %mixw.1, f32[1,1280]{1,0:T(1,128)} %bias.1, f32[1,2048]{1,0:T(1,128)} %bitcast.1, ...), custom_call_target="tpu_custom_call" | custom-call | tf_op jit(solution)/shard_map/gating/pallas_call | solution.py:579
  77.5 1.1 %copy.10 = bf16[1,320,2048]{2,1,0:T(8,128)(2,1)} copy(bf16[1,320,2048]{2,1,0:T(8,128)(2,1)S(1)} %gating.1) | data formatting | bytes 2621440
